TPU v7x, 32 devices: a whole 2x2x4 slice. The times are simulated.
32 devices in a mesh: ep: 8 (over z, core), tp: 4 (over y, x).
Axes of the slice: x: 2, y: 2, z: 4, core: 2. Of those that a mesh axis runs over, the one named last changes fastest.
Arguments:
- queries: bfloat16 [4096, 1024], P('ep', 'tp'), may hold values from -9 to 9
- keys: bfloat16 [4096, 128], P('ep'), may hold values from -6 to 6
- values: bfloat16 [4096, 128], P('ep'), may hold values from -6 to 6
- sink_logits: float32 [16], P('tp'), may hold values from 2 to 7
- out_weight: bfloat16 [1024, 2048], P(None, 'tp'), may hold values from -0.8984375 to 0.8984375
- expert_input: bfloat16 [2048, 2048], P('ep'), may hold values from -6 to 6
- norm_gain: float32 [2048], replicated, may hold values from 0.1 to 1.9
- routes: int32 [2048, 2], P('ep'), may hold values from 0 to 7, all different within a row; in each aligned block of 256 rows (0 to 255, 256 to 511, ...) at most 128 rows name the same one
- route_weights: float32 [2048, 2], P('ep'), may hold values from 0.1 to 1
- gate_weight: bfloat16 [8, 2048, 4096], P('ep', None, 'tp'), may hold values from -0.125 to 0.125
- up_weight: bfloat16 [8, 2048, 4096], P('ep', None, 'tp'), may hold values from -0.125 to 0.125
- down_weight: bfloat16 [8, 4096, 2048], P('ep', 'tp'), may hold values from -0.09375 to 0.09375
Outputs:
- attn_out: bfloat16 [4096, 2048], P('ep', 'tp')
- expert_out: bfloat16 [2048, 2048], P('ep', 'tp')
Inputs may be any that keep to these rules, and one draw needn't show every extreme that they name: `routes`: each row names 2 different experts. Within the rows of one index of ep (aligned blocks of 256 rows) no expert is named by more than 128 rows, and in some blocks one expert is named by exactly 128 rows.
All inputs are finite; a program needn't handle non-finite values.
Results may differ from a plain program's by a relative error of at most 0.015.
Values may be sent and summed in bfloat16 or wider, within the bound.
No kernel may reach another device: no remote copies, remote signals or barrier semaphores. Data moves between devices by JAX's collectives and lax.ppermute only.
A program may use at most 64 MiB of HBM per device.

v0:
```python
import jax
import jax.numpy as jnp
from jax import lax
from jax.sharding import PartitionSpec as P

HEADS = 16
KV = 2
HD = 64
WINDOW = 128


rms_eps = 1e-06
mask_value = -1e30


def passed_along(value, axis, steps):
    count = lax.axis_size(axis)
    first, last = (max(0, -steps), min(count, count - steps))
    return lax.ppermute(value, axis, [(source, source + steps) for source in range(first, last)])


def rotate_heads(values_in, positions):
    half_dim = values_in.shape[-1] // 2
    inv_freq = 10000.0 ** (-jnp.arange(half_dim, dtype=jnp.float32) * (2.0 / values_in.shape[-1]))
    angles = positions[:, None] * inv_freq[None, :]
    cosine_table = jnp.cos(angles)[:, None, :]
    sine_table = jnp.sin(angles)[:, None, :]
    first_half = values_in[..., :half_dim]
    second_half = values_in[..., half_dim:]
    return jnp.concatenate(
        [
            first_half * cosine_table - second_half * sine_table,
            second_half * cosine_table + first_half * sine_table,
        ],
        axis=-1,
    )


def local(
    queries,
    keys,
    values,
    sink_logits,
    out_weight,
    expert_input,
    norm_gain,
    routes,
    route_weights,
    gate_weight,
    up_weight,
    down_weight,
):
    seq_rows = queries.shape[0]
    heads_here = queries.shape[1] // HD
    group_size = HEADS // KV
    kv_here = max(1, heads_here // group_size)
    heads_per_kv = heads_here // kv_here
    kv_first = lax.axis_index("tp") * heads_here // group_size
    key_local = lax.dynamic_slice_in_dim(keys, kv_first * HD, kv_here * HD, 1)
    value_local = lax.dynamic_slice_in_dim(values, kv_first * HD, kv_here * HD, 1)
    offset = lax.axis_index("ep") * seq_rows
    positions = (offset + jnp.arange(seq_rows, dtype=jnp.int32)).astype(jnp.float32)
    query_rot = rotate_heads(
        queries.astype(jnp.float32).reshape(seq_rows, heads_here, HD), positions
    ).astype(jnp.bfloat16)
    key_rot = rotate_heads(
        key_local.astype(jnp.float32).reshape(seq_rows, kv_here, HD), positions
    ).astype(jnp.bfloat16)
    value_heads = value_local.reshape(seq_rows, kv_here, HD)
    rim_pair = jnp.concatenate(
        [
            key_rot.reshape(seq_rows, kv_here * HD)[seq_rows - WINDOW :],
            value_local[seq_rows - WINDOW :],
        ],
        axis=1,
    )
    rim_pair = passed_along(rim_pair, "ep", 1)
    rim_key = rim_pair[:, : kv_here * HD].reshape(WINDOW, kv_here, HD)
    rim_value = rim_pair[:, kv_here * HD :].reshape(WINDOW, kv_here, HD)
    blocks = seq_rows // WINDOW

    def band_of(rim_part, local_part):
        padded = jnp.concatenate([rim_part, local_part], axis=0)
        earlier = padded[:seq_rows].reshape(blocks, WINDOW, kv_here, HD)
        current = padded[WINDOW:].reshape(blocks, WINDOW, kv_here, HD)
        return jnp.concatenate([earlier, current], axis=1)

    key_band = band_of(rim_key, key_rot)
    value_band = band_of(rim_value, value_heads)
    query_blocks = query_rot.reshape(blocks, WINDOW, kv_here, heads_per_kv, HD)
    scores = jnp.einsum(
        "nqhgd,nkhd->nhgqk", query_blocks, key_band, preferred_element_type=jnp.float32
    ) * HD ** (-0.5)
    block_start = offset + jnp.arange(blocks, dtype=jnp.int32)[:, None, None] * WINDOW
    query_pos = block_start + jnp.arange(WINDOW, dtype=jnp.int32)[None, :, None]
    key_pos = block_start - WINDOW + jnp.arange(2 * WINDOW, dtype=jnp.int32)[None, None, :]
    distance = query_pos - key_pos
    allowed = (distance >= 0) & (distance < WINDOW) & (key_pos >= 0)
    scores = jnp.where(allowed[:, None, None], scores, mask_value)
    sink_row = sink_logits.reshape(1, kv_here, heads_per_kv, 1)
    row_top = jnp.maximum(jnp.max(scores, axis=-1), sink_row)
    exp_scores = jnp.exp(scores - row_top[..., None])
    row_total = jnp.sum(exp_scores, axis=-1) + jnp.exp(sink_row - row_top)
    weights = (exp_scores / row_total[..., None]).astype(jnp.bfloat16)
    head_mix = jnp.einsum(
        "nhgqk,nkhd->nqhgd", weights, value_band, preferred_element_type=jnp.float32
    )
    head_mix = head_mix.astype(jnp.bfloat16).reshape(seq_rows, heads_here * HD)
    attn_out = jnp.dot(
        lax.all_gather(head_mix, "tp", axis=1, tiled=True),
        out_weight,
        preferred_element_type=jnp.float32,
    ).astype(jnp.bfloat16)
    token_rows = expert_input.shape[0]
    top_count = routes.shape[1]
    expert_count = lax.axis_size("ep")
    capacity = 2 * top_count * token_rows // expert_count
    slot_total = expert_count * capacity
    input_wide = expert_input.astype(jnp.float32)
    inv_rms = lax.rsqrt(jnp.mean(input_wide * input_wide, axis=-1, keepdims=True) + rms_eps)
    normed = (input_wide * inv_rms * norm_gain[None, :]).astype(jnp.bfloat16)
    flat_expert = routes.reshape(-1)
    one_hot = (flat_expert[:, None] == jnp.arange(expert_count, dtype=jnp.int32)[None, :]).astype(
        jnp.int32
    )
    route_rank = jnp.sum(jnp.cumsum(one_hot, axis=0) * one_hot, axis=1) - 1
    slot_of_route = flat_expert * capacity + route_rank
    matches = slot_of_route[None, :] == jnp.arange(slot_total, dtype=jnp.int32)[:, None]
    route_token = jnp.arange(token_rows * top_count, dtype=jnp.int32) // top_count
    source_row = jnp.sum(jnp.where(matches, route_token[None, :] + 1, 0), axis=1) - 1
    occupied = source_row >= 0
    gate_local = gate_weight[0]
    up_local = up_weight[0]
    down_local = down_weight[0]
    column_count = normed.shape[1] // lax.axis_size("tp")
    own_columns = lax.dynamic_slice_in_dim(
        normed, lax.axis_index("tp") * column_count, column_count, 1
    )
    slot_rows = jnp.where(
        occupied[:, None],
        jnp.take(own_columns, jnp.maximum(source_row, 0), axis=0),
        jnp.zeros((), jnp.bfloat16),
    )
    outgoing = slot_rows.reshape(expert_count, capacity, column_count)
    arrived = lax.all_to_all(outgoing, "ep", split_axis=0, concat_axis=0, tiled=True)
    leading = arrived.shape[:2]
    portion = lax.all_gather(arrived, "tp", axis=2, tiled=True)
    flat_piece = portion.reshape(-1, portion.shape[2])
    gate_acc = jnp.dot(flat_piece, gate_local, preferred_element_type=jnp.float32)
    up_acc = jnp.dot(flat_piece, up_local, preferred_element_type=jnp.float32)
    hidden = (jax.nn.silu(gate_acc) * up_acc).astype(jnp.bfloat16)
    summed = lax.psum_scatter(
        lax.dot_general(
            down_local, hidden, (((0,), (1,)), ((), ())), preferred_element_type=jnp.float32
        ).astype(jnp.bfloat16),
        "tp",
        scatter_dimension=0,
        tiled=True,
    ).astype(jnp.float32)
    returned = summed.astype(jnp.bfloat16).reshape((summed.shape[0],) + leading)
    results_home = lax.all_to_all(returned, "ep", split_axis=1, concat_axis=1, tiled=True)
    home_flat = results_home.reshape(results_home.shape[0], -1)
    picked = jnp.take(home_flat, slot_of_route, axis=1).astype(jnp.float32)
    weighted = picked * route_weights.reshape(1, -1)
    combined = jnp.sum(weighted.reshape(results_home.shape[0], token_rows, top_count), axis=2)
    expert_out = combined.T.astype(jnp.bfloat16)
    return (attn_out, expert_out)


def solution(mesh):
    return jax.shard_map(
        local,
        mesh=mesh,
        in_specs=(
            P("ep", "tp"),
            P("ep", None),
            P("ep", None),
            P("tp"),
            P(None, "tp"),
            P("ep", None),
            P(),
            P("ep", None),
            P("ep", None),
            P("ep", None, "tp"),
            P("ep", None, "tp"),
            P("ep", "tp", None),
        ),
        out_specs=(P("ep", "tp"), P("ep", "tp")),
        check_vma=False,
    )
```

profile of v0, /device:TPU:0, one launch (start us, length us, event | category | flops | bytes accessed | tf_op | source)
XLA Modules:
  0.0 217.6 jit_solution(8200057702894979410)
XLA Ops:
  7.2 1.5 convert_element_type.82
  8.8 1.5 multiply_reduce_fusion
  10.7 1.1 reduce-window.6
  11.9 0.2 slice_reduce_fusion
  12.2 0.3 select_reduce_fusion
  12.6 0.8 dynamic-slice
  13.5 4.0 %gather_fusion = bf16[1024,512]{1,0:T(8,128)(2,1)S(1)} fusion(bf16[256,512]{1,0:T(8,128)(2,1)S(1)} %fusion.14, s32[1024]{0:T(1024)S(1)} %maximum_clamp_fusion), kind=kCustom, calls=%fused_computation | custom fusion | bytes 2101248 | tf_op jit(solution)/shard_map/jit(_take)/gather | solution.py:141
  17.5 0.5 select_select_fusion
  17.9 32.8 %all_to_all.10 = bf16[8,128,512]{2,1,0:T(8,128)(2,1)} all-to-all(bf16[8,128,512]{2,1,0:T(8,128)(2,1)S(1)} %select_select_fusion), channel_id=1, replica_groups=mesh['ep'=8,'tp'=4] {'ep'}, dimensions={0} | all-to-all | bytes 2097152 | tf_op jit(solution)/shard_map/all_to_all | solution.py:145
  50.8 51.5 %all-gather.5.cloned.1.call-done = bf16[8,128,2048]{2,1,0:T(8,128)(2,1)} async-done(((bf16[8,128,512]{2,1,0:T(8,128)(2,1)}), bf16[8,128,2048]{2,1,0:T(8,128)(2,1)}) %all-gather.5.cloned.1.call-update) | async-done | bytes 4194320 | tf_op jit(solution)/shard_map/all_gather | solution.py:147
  102.3 7.6 %fusion.2 = f32[1024,1024]{1,0:T(8,128)S(1)} fusion(bf16[1024,2048]{1,0:T(8,128)(2,1)} %bitcast.127, bf16[1,2048,1024]{2,1,0:T(8,128)(2,1)} %param.22), kind=kOutput, calls=%fused_computation.4 | convolution fusion | flops 4294967296 | bytes 12582912 | tf_op jit(solution)/shard_map/dot_general | solution.py:150
  110.0 5.4 %multiply_convert_fusion = bf16[1024,1024]{1,0:T(8,128)(2,1)S(1)} fusion(f32[1024,1024]{1,0:T(8,128)S(1)} %fusion.2, bf16[1024,2048]{1,0:T(8,128)(2,1)S(1)} %bitcast.128, bf16[1,2048,1024]{2,1,0:T(8,128)(2,1)S(1)} %copy-done.7), kind=kOutput, calls=%fused_computation.9 | convolution fusion | flops 4301258752 | bytes 14680064 | tf_op jit(solution)/shard_map/dot_general | solution.py:149
  115.4 6.1 %convert_bitcast_fusion = bf16[2048,1024]{0,1:T(8,128)(2,1)} fusion(bf16[1024,1024]{1,0:T(8,128)(2,1)S(1)} %multiply_convert_fusion, bf16[1,1024,2048]{2,1,0:T(8,128)(2,1)S(1)} %copy-done.8), kind=kOutput, calls=%fused_computation.8 | convolution fusion | flops 4297064448 | bytes 10485760 | tf_op jit(solution)/shard_map/dot_general | solution.py:153
  121.5 0.8 copy-done.2
  122.8 0.3 fusion.33
  123.2 1.6 collective-permute-start
  125.2 0.3 multiply_cosine_fusion
  125.5 0.3 fusion.16
  126.1 0.5 fusion.47
  126.7 0.3 fusion.10
  127.1 0.5 fusion.11
  127.6 0.2 copy.79
  127.8 0.7 copy.105
  128.6 45.6 %reduce-scatter.2.cloned.1.call-done = bf16[512,1024]{0,1:T(8,128)(2,1)} async-done(((bf16[2048,1024]{0,1:T(8,128)(2,1)}), bf16[512,1024]{0,1:T(8,128)(2,1)}) %reduce-scatter.2.cloned.1.call-update) | async-done | bytes 1048592 | tf_op jit(solution)/shard_map/reduce_scatter | solution.py:152
  174.2 4.6 %all-to-all-start.1 = ((bf16[512,8,128]{0,2,1:T(8,128)(2,1)}), bf16[512,8,128]{0,2,1:T(8,128)(2,1)S(1)}, u32[]{:S(2)}, u32[]{:S(2)}) async-start(bf16[512,8,128]{0,2,1:T(8,128)(2,1)} %bitcast.120), calls=%async_computation.2 | async-start | bytes 2097152 | tf_op jit(solution)/shard_map/all_to_all | solution.py:161
  179.0 0.1 mul.228
  179.4 0.2 copy.83
  179.7 23.4 %all-gather.3.cloned.1.call-done = bf16[512,1024]{0,1:T(8,128)(2,1)} async-done(((bf16[512,256]{0,1:T(8,128)(2,1)}), bf16[512,1024]{0,1:T(8,128)(2,1)}) %all-gather.3.cloned.1.call-update) | async-done | bytes 1048592 | tf_op jit(solution)/shard_map/all_gather | solution.py:110
  203.2 2.8 %convolution_convert_fusion = bf16[512,512]{1,0:T(8,128)(2,1)} fusion(bf16[512,1024]{0,1:T(8,128)(2,1)} %all-gather.3.cloned.1.call-done, bf16[1024,512]{1,0:T(8,128)(2,1)S(1)} %copy-done), kind=kOutput, calls=%fused_computation.17 | convolution fusion | flops 537133056 | bytes 2621440 | tf_op jit(solution)/shard_map/dot_general | solution.py:109
  205.9 2.0 gather_fusion.1
  207.9 0.2 gather.15
  208.1 2.9 %multiply_reduce_fusion.1 = bf16[512,256]{0,1:T(8,128)(2,1)} fusion(bf16[512,256,2]{0,2,1:T(2,128)(2,1)S(1)} %gather.15, pred[256,2]{1,0:T(8,128)(4,1)S(1)} %copy.83, f32[256,2]{1,0:T(8,128)S(1)} %copy.85), kind=kLoop, calls=%fused_computation.21 | loop fusion | flops 917504 | bytes 788992 | tf_op jit(solution)/shard_map/reduce_sum | solution.py:165
  (73 shorter events, 2.6 us)
Async XLA Ops:
  7.2 196.0 %copy-start = (bf16[1024,512]{1,0:T(8,128)(2,1)S(1)}, bf16[1024,512]{1,0:T(8,128)(2,1)}, u32[]{:S(2)}) copy-start(bf16[1024,512]{1,0:T(8,128)(2,1)} %param.16) | copy-start | bytes 3145732
  7.2 3.1 %copy-start.4 = (s32[256,2]{0,1:T(2,128)S(1)}, s32[256,2]{0,1:T(2,128)}, u32[]{:S(2)}) copy-start(s32[256,2]{0,1:T(2,128)} %param.19) | copy-start | bytes 6148
  7.2 95.1 %all-gather.5.cloned.1.call-start = ((), (), s32[]{:S(2)}) async-start(), calls=%async_computation.4 | async-start | bytes 5242880 | tf_op jit(solution)/shard_map/all_gather | solution.py:147
  50.8 123.5 %reduce-scatter.2.cloned.1.call-start = ((), (), s32[]{:S(2)}) async-start(), calls=%async_computation.5 | async-start | bytes 5242880 | tf_op jit(solution)/shard_map/reduce_scatter | solution.py:152
  102.3 7.7 %copy-start.7 = (bf16[1,2048,1024]{2,1,0:T(8,128)(2,1)S(1)}, bf16[1,2048,1024]{2,1,0:T(8,128)(2,1)}, u32[]{:S(2)}) copy-start(bf16[1,2048,1024]{2,1,0:T(8,128)(2,1)} %param.21) | copy-start | bytes 12582916
  102.3 7.7 %copy-start.9 = (bf16[8,128,2048]{2,1,0:T(8,128)(2,1)S(1)}, bf16[8,128,2048]{2,1,0:T(8,128)(2,1)}, u32[]{:S(2)}) copy-start(bf16[8,128,2048]{2,1,0:T(8,128)(2,1)} %all-gather.5.cloned.1.call-done) | copy-start | bytes 12582916
  110.0 5.4 %copy-start.8 = (bf16[1,1024,2048]{2,1,0:T(8,128)(2,1)S(1)}, bf16[1,1024,2048]{2,1,0:T(8,128)(2,1)}, u32[]{:S(2)}) copy-start(bf16[1,1024,2048]{2,1,0:T(8,128)(2,1)} %param.23) | copy-start | bytes 12582916
  121.4 0.9 copy-start.2
  121.4 1.0 copy-start.3
  121.4 3.3 %copy-start.1 = (bf16[512,256]{1,0:T(8,128)(2,1)S(1)}, bf16[512,256]{1,0:T(8,128)(2,1)}, u32[]{:S(2)}) copy-start(bf16[512,256]{1,0:T(8,128)(2,1)} %param.12) | copy-start | bytes 786436
  121.5 5.2 %copy-start.6 = (f32[4]{0:T(128)S(1)}, f32[4]{0:T(128)}, u32[]{:S(2)}) copy-start(f32[4]{0:T(128)} %param.15) | copy-start | bytes 52
  121.5 81.7 %all-gather.3.cloned.1.call-start = ((), (), s32[]{:S(2)}) async-start(), calls=%async_computation.3 | async-start | bytes 1310720 | tf_op jit(solution)/shard_map/all_gather | solution.py:110
  123.2 2.9 %collective-permute-start = (bf16[128,128]{0,1:T(8,128)(2,1)S(1)}, bf16[128,128]{0,1:T(8,128)(2,1)S(1)}, u32[]{:S(2)}, u32[]{:S(2)}) collective-permute-start(bf16[128,128]{0,1:T(8,128)(2,1)S(1)} %pad_maximum_fusion.3), channel_id=1, source_target_pairs={{0,4},{4,8},{8,12},{12,16},{16,20},{20,24},{24,28},{1,5},{5,9},{9,... | collective-permute-start | bytes 98312 | tf_op jit(solution)/shard_map/ppermute | solution.py:19
  127.1 52.5 %copy-start.5 = (f32[256,2]{0,1:T(2,128)S(1)}, f32[256,2]{0,1:T(2,128)}, u32[]{:S(2)}) copy-start(f32[256,2]{0,1:T(2,128)} %param.20) | copy-start | bytes 6148
  174.2 31.7 %all-to-all-start.1 = ((bf16[512,8,128]{0,2,1:T(8,128)(2,1)}), bf16[512,8,128]{0,2,1:T(8,128)(2,1)S(1)}, u32[]{:S(2)}, u32[]{:S(2)}) async-start(bf16[512,8,128]{0,2,1:T(8,128)(2,1)} %bitcast.120), calls=%async_computation.2 | async-start | bytes 2097152 | tf_op jit(solution)/shard_map/all_to_all | solution.py:161
Sparse Core Ops, SparseCore 0:
  50.9 51.3 all-gather.4
  121.6 52.5 reduce-scatter.1
  176.6 26.4 all-gather.2
where the time goes:
time: 218 us
  waiting for transfers between devices  121 us (56%)
  blocking collectives  32.8 us (15%)
  matrix products  22.8 us (10%)
  between operations  14.2 us (7%)
  local copies, waits for them, and re-layouts  10.8 us (5%)
  other arithmetic  10 us (5%)
  starting transfers between devices  6.3 us (3%)
    all_gather x1, waiting for transfers between devices, local(): portion = lax.all_gather(arrived, 'tp', axis=2, tiled=True)  51.5 us
    reduce_scatter x1, waiting for transfers between devices, local(): lax.psum_scatter(lax.dot_general(down_local, hidden, (((0,), (1,)), ((),...  45.6 us
    all_to_all x1, blocking collectives, local(): lax.all_to_all(outgoing, 'ep', split_axis=0, concat_axis=0, tiled=True)  32.8 us
    all_gather x1, waiting for transfers between devices, local(): lax.all_gather(head_mix, 'tp', axis=1, tiled=True)  23.4 us
    dot_general x1, matrix products, local(): up_acc = jnp.dot(flat_piece, up_local, preferred_element_type=jnp.float32)  7.64 us
    dot_general x1, matrix products, local(): lax.dot_general(down_local, hidden, (((0,), (1,)), ((), ())), preferred_e...  6.07 us
    dot_general x1, matrix products, local(): jnp.dot(flat_piece, gate_local, preferred_element_type=jnp.float32)  5.35 us
    all_to_all x1, starting transfers between devices, local(): lax.all_to_all(returned, 'ep', split_axis=1, concat_axis=1, tiled=True)  4.61 us
  transfers between devices with their start and end apart: 5, of which 3 were waited for; matrix products, arithmetic and copies ran while one was open for 4% of the time, Pallas kernels for 0%

commit v1 on v0

--- a/solution.py
+++ b/solution.py
@@ -1,7 +1,13 @@
+import functools
+
 import jax
 import jax.numpy as jnp
+import numpy as np
 from jax import lax
+from jax.experimental import pallas as pl
+from jax.experimental.pallas import tpu as pltpu
 from jax.sharding import PartitionSpec as P
+
 
 HEADS = 16
 KV = 2
@@ -36,7 +42,7 @@
     )
 
 
-def local(
+def local_general(
     queries,
     keys,
     values,
@@ -167,9 +173,538 @@
     return (attn_out, expert_out)
 
 
+BF = jnp.bfloat16
+F32 = jnp.float32
+MIB = 1024 * 1024
+LATE = 2
+NEAR = 1
+
+
+def dot(left, right):
+    return jnp.dot(left, right, preferred_element_type=F32)
+
+
+def quarter(index, width):
+    return pl.ds(pl.multiple_of(index * width, width), width)
+
+
+def kernel_params(limit_mib, **extra):
+    return pltpu.CompilerParams(vmem_limit_bytes=limit_mib * MIB, **extra)
+
+
+def in_hbm(*values):
+    return [pltpu.with_memory_space_constraint(value, pltpu.HBM) for value in values]
+
+
+def whole_specs(count):
+    return [pl.BlockSpec(memory_space=pltpu.VMEM)] * count
+
+
+def axes_here():
+    first = 1 + lax.rem(lax.axis_index("ep"), 2)
+    return first, 3 - first
+
+
+def naming(routes, lanes):
+    choices, tokens = routes.shape
+    expert = lax.broadcasted_iota(jnp.int32, (lanes, tokens), 0)
+    hit = routes[0:1, :] == expert
+    for choice in range(1, choices):
+        hit = hit | (routes[choice : choice + 1, :] == expert)
+    named = jnp.where(hit, 1.0, 0.0).astype(BF)
+    row = lax.broadcasted_iota(jnp.int32, (tokens, tokens), 0)
+    column = lax.broadcasted_iota(jnp.int32, (tokens, tokens), 1)
+    earlier = jnp.where(row < column, 1.0, 0.0).astype(BF)
+    return jnp.where(hit, dot(named, earlier), -1.0)
+
+
+def dispatch_kernel(capacity, chips, x_hbm, gain_hbm, routes_hbm, queries_hbm, keys_hbm, values_hbm, *refs):
+    outs, (x, gain, routes, normed, slot_of, arrival) = refs[:-6], refs[-6:]
+    lanes = keys_hbm.shape[1]
+    tail = pl.ds(keys_hbm.shape[0] - WINDOW, WINDOW)
+    rim, queries, keys, values = outs[-4:]
+    moves = (
+        (routes_hbm, routes),
+        (x_hbm, x),
+        (gain_hbm, gain),
+        (keys_hbm.at[tail, :], rim.at[:, :lanes]),
+        (values_hbm.at[tail, :], rim.at[:, lanes:]),
+        (queries_hbm, queries),
+        (keys_hbm, keys),
+        (values_hbm, values),
+    )
+    copies = [pltpu.make_async_copy(s, d, arrival.at[i]) for i, (s, d) in enumerate(moves)]
+    for copy in copies:
+        copy.start()
+    me = lax.axis_index("ep")
+    chip, core = me // 2, lax.rem(me, 2)
+    tokens = x.shape[0]
+    copies[0].wait()
+    slot_of[...] = naming(routes[...], slot_of.shape[0])
+    copies[1].wait()
+    copies[2].wait()
+    wide = x[...].astype(F32)
+    inv_rms = lax.rsqrt(jnp.mean(wide * wide, axis=-1, keepdims=True) + rms_eps)
+    normed[...] = (wide * inv_rms * gain[...]).astype(BF)
+    slot = lax.broadcasted_iota(jnp.int32, (capacity, tokens), 0).astype(F32)
+
+    def chosen(expert):
+        return jnp.where(slot_of[pl.ds(expert, 1), :] == slot, 1.0, 0.0).astype(BF)
+
+    width = outs[0].shape[1]
+    share = normed[:, quarter(lax.axis_index("tp"), width)]
+    place = 0
+    for step in range(chips - 1, -1, -1):
+        for other in range(2):
+            rows = share if step > NEAR else normed[...]
+            expert = (chip ^ step) * 2 + (core ^ other)
+            outs[place][...] = dot(chosen(expert), rows).astype(BF)
+            place += 1
+    for copy in copies[3:]:
+        copy.wait()
+
+
+def dispatch(x, gain, routes, queries, keys, values, capacity, chips, width):
+    tokens, features = x.shape
+    shapes = [(capacity, width if i < 2 * (chips - 1 - NEAR) else features) for i in range(2 * chips)]
+    shapes += [(WINDOW, 2 * keys.shape[1]), queries.shape, keys.shape, values.shape]
+    return pl.pallas_call(
+        functools.partial(dispatch_kernel, capacity, chips),
+        out_shape=[jax.ShapeDtypeStruct(s, BF) for s in shapes],
+        in_specs=[pl.BlockSpec(memory_space=pltpu.HBM)] * 6,
+        out_specs=whole_specs(len(shapes)),
+        scratch_shapes=[
+            pltpu.VMEM((tokens, features), BF),
+            pltpu.VMEM((1, features), F32),
+            pltpu.VMEM(routes.shape[::-1], jnp.int32),
+            pltpu.VMEM((tokens, features), BF),
+            pltpu.VMEM((8 * -(-2 * chips // 8), tokens), F32),
+            pltpu.SemaphoreType.DMA((8,)),
+        ],
+        compiler_params=kernel_params(24),
+        cost_estimate=pl.CostEstimate(
+            flops=4 * capacity * tokens * features * 2, bytes_accessed=4 * MIB, transcendentals=0
+        ),
+        name="dispatch",
+    )(*in_hbm(x, gain.reshape(1, -1), routes.T, queries, keys, values))
+
+
+def experts_kernel(split, fetch, blocks, *refs):
+    count = 4 if split else 2
+    rows_in = refs[:count]
+    x, hidden = refs[-2:]
+    if not fetch:
+        gate, up, down, mine_ref, second_ref, far_ref = refs[count:-2]
+    else:
+        gate_hbm, up_hbm, down_hbm, gate, up, down, mine_ref, second_ref, far_ref, arrival = refs[count:-2]
+    here = lax.axis_index("tp")
+    first, second = axes_here()
+    width = mine_ref.shape[1]
+    block = hidden.shape[1] // blocks
+    parts = [pl.ds(step * block, block) for step in range(blocks)]
+    quarters = [quarter(index, width) for index in (here ^ first, here ^ 3, here ^ second, here)]
+    copies = []
+    if fetch:
+        for place, part in enumerate(parts):
+            for source, target, row in ((gate_hbm, gate, 0), (up_hbm, up, 1)):
+                copies.append(
+                    pltpu.make_async_copy(
+                        source.at[:, :, part], target.at[:, :, part], arrival.at[row, place]
+                    )
+                )
+        for place, part in enumerate(quarters):
+            copies.append(
+                pltpu.make_async_copy(down_hbm.at[:, :, part], down.at[:, :, part], arrival.at[2, place])
+            )
+        for copy in copies:
+            copy.start()
+    if split:
+        for ref, index in zip(rows_in, (here, here ^ first, here ^ second, here ^ 3)):
+            x[:, quarter(index, width)] = ref[...]
+    else:
+        half = rows_in[0].shape[0]
+        x[:half, :] = rows_in[0][...]
+        x[half:, :] = rows_in[1][...]
+    for place, part in enumerate(parts):
+        for copy in copies[2 * place : 2 * place + 2]:
+            copy.wait()
+        gated = dot(x[...], gate[0, :, part])
+        upped = dot(x[...], up[0, :, part])
+        hidden[:, part] = (gated / (1.0 + jnp.exp(-gated)) * upped).astype(BF)
+    for place, part in enumerate(quarters):
+        for copy in copies[2 * blocks + place : 2 * blocks + place + 1]:
+            copy.wait()
+        product = dot(hidden[...], down[0, :, part]).astype(BF)
+        if place < 2:
+            far_ref[:, place * width : (place + 1) * width] = product
+        else:
+            (second_ref if place == 2 else mine_ref)[...] = product
+
+
+def experts(rows_in, weights, width, blocks, fetch=False):
+    split = len(rows_in) == 4
+    rows = rows_in[0].shape[0] if split else 2 * rows_in[0].shape[0]
+    _, features, hidden = weights[0].shape
+    out_shape = [
+        jax.ShapeDtypeStruct((rows, width), BF),
+        jax.ShapeDtypeStruct((rows, width), BF),
+        jax.ShapeDtypeStruct((rows, 2 * width), BF),
+    ]
+    scratch = [pltpu.VMEM((rows, features), BF), pltpu.VMEM((rows, hidden), BF)]
+    weight_specs = whole_specs(3)
+    if fetch:
+        weights = in_hbm(*weights)
+        out_shape = [jax.ShapeDtypeStruct(w.shape, w.dtype) for w in weights] + out_shape
+        weight_specs = [pl.BlockSpec(memory_space=pltpu.HBM)] * 3
+        scratch = [pltpu.SemaphoreType.DMA((3, max(4, blocks)))] + scratch
+    return pl.pallas_call(
+        functools.partial(experts_kernel, split, fetch, blocks),
+        out_shape=out_shape,
+        in_specs=whole_specs(len(rows_in)) + weight_specs,
+        out_specs=whole_specs(len(out_shape)),
+        scratch_shapes=scratch,
+        compiler_params=kernel_params(24 if fetch else 8),
+        cost_estimate=pl.CostEstimate(
+            flops=6 * rows * features * hidden,
+            bytes_accessed=6 * features * hidden,
+            transcendentals=rows * hidden,
+        ),
+        name="experts",
+    )(*rows_in, *weights)
+
+
+def join_kernel(top_ref, bottom_ref, out_ref):
+    rows = top_ref.shape[0]
+    out_ref[:rows, :] = top_ref[...]
+    out_ref[rows:, :] = bottom_ref[...]
+
+
+def join(top, bottom):
+    rows, columns = top.shape
+    return pl.pallas_call(
+        join_kernel,
+        out_shape=jax.ShapeDtypeStruct((2 * rows, columns), top.dtype),
+        in_specs=whole_specs(2),
+        out_specs=pl.BlockSpec(memory_space=pltpu.VMEM),
+        compiler_params=kernel_params(2),
+        cost_estimate=pl.CostEstimate(flops=MIB, bytes_accessed=MIB, transcendentals=0),
+        name="join",
+    )(top, bottom)
+
+
+def settle_kernel(mine_ref, near_ref, last_ref, same_ref, cross_ref):
+    rows, width = same_ref.shape
+    for out_ref, start in ((same_ref, 0), (cross_ref, rows)):
+        part = pl.ds(start, rows)
+        total = mine_ref[part, :].astype(F32) + near_ref[part, :width].astype(F32)
+        out_ref[...] = (total + last_ref[part, :].astype(F32)).astype(BF)
+
+
+def settle(mine, near, last):
+    rows, width = mine.shape
+    return pl.pallas_call(
+        settle_kernel,
+        out_shape=[jax.ShapeDtypeStruct((rows // 2, width), BF)] * 2,
+        in_specs=whole_specs(3),
+        out_specs=whole_specs(2),
+        compiler_params=kernel_params(4),
+        cost_estimate=pl.CostEstimate(flops=MIB, bytes_accessed=MIB, transcendentals=0),
+        name="settle",
+    )(mine, near, last)
+
+
+def project_kernel(*refs):
+    parts, (weight_ref, out_ref) = refs[:4], refs[4:]
+    here = lax.axis_index("tp")
+    first, second = axes_here()
+    depth = parts[0].shape[1]
+    total = None
+    for ref, index in zip(parts, (here, here ^ first, here ^ second, here ^ 3)):
+        term = dot(ref[...], weight_ref[quarter(index, depth), :])
+        total = term if total is None else total + term
+    out_ref[...] = total.astype(BF)
+
+
+def project(parts, weight):
+    rows, columns = parts[0].shape[0], weight.shape[1]
+    return pl.pallas_call(
+        project_kernel,
+        out_shape=jax.ShapeDtypeStruct((rows, columns), BF),
+        in_specs=whole_specs(5),
+        out_specs=pl.BlockSpec(memory_space=pltpu.VMEM),
+        compiler_params=kernel_params(8),
+        cost_estimate=pl.CostEstimate(
+            flops=2 * rows * weight.shape[0] * columns, bytes_accessed=3 * MIB, transcendentals=0
+        ),
+        name="project",
+    )(*parts, weight)
+
+
+def combine_kernel(steps, late, *refs):
+    routes_ref, weights_ref = refs[:2]
+    pieces, (sum_ref, high_ref, low_ref) = refs[2:-3], refs[-3:]
+    me = lax.axis_index("ep")
+    chip, core = me // 2, lax.rem(me, 2)
+    routes = routes_ref[...]
+    choices, tokens = routes.shape
+    capacity = high_ref.shape[1] // (2 * late)
+    slot_of = naming(routes, 128)
+    row = lax.broadcasted_iota(jnp.int32, (128, tokens), 0)
+    scale = jnp.zeros((128, tokens), F32)
+    for choice in range(choices):
+        scale = jnp.where(routes[choice : choice + 1, :] == row, weights_ref[choice : choice + 1, :], scale)
+    slot_of = slot_of.T.astype(BF)
+    scale = scale.T
+    high = scale.astype(BF)
+    low = (scale - high.astype(F32)).astype(BF)
+    slot = lax.broadcasted_iota(jnp.int32, (tokens, capacity), 1).astype(F32)
+    source = lax.broadcasted_iota(jnp.int32, (128, capacity), 0)
+    total = None
+    for place in range(2 * len(steps)):
+        expert = (chip ^ steps[place // 2]) * 2 + (core ^ (place % 2))
+        pick = jnp.where(source == expert, 1.0, 0.0).astype(BF)
+        taken = dot(slot_of, pick) == slot
+        spread = [jnp.where(taken, dot(scales, pick), 0.0).astype(BF) for scales in (high, low)]
+        if place < len(pieces):
+            for part in spread:
+                term = dot(part, pieces[place][...])
+                total = term if total is None else total + term
+        else:
+            column = (place - len(pieces)) * capacity
+            high_ref[:, column : column + capacity] = spread[0]
+            low_ref[:, column : column + capacity] = spread[1]
+    sum_ref[...] = total
+
+
+def combine(routes, weights, steps, late, pieces):
+    tokens, columns = routes.shape[0], pieces[0].shape[1]
+    capacity = pieces[0].shape[0]
+    return pl.pallas_call(
+        functools.partial(combine_kernel, steps, late),
+        out_shape=[
+            jax.ShapeDtypeStruct((tokens, columns), F32),
+            jax.ShapeDtypeStruct((tokens, 2 * late * capacity), BF),
+            jax.ShapeDtypeStruct((tokens, 2 * late * capacity), BF),
+        ],
+        in_specs=whole_specs(2 + len(pieces)),
+        out_specs=whole_specs(3),
+        compiler_params=kernel_params(8),
+        cost_estimate=pl.CostEstimate(
+            flops=4 * len(pieces) * tokens * capacity * columns,
+            bytes_accessed=2 * MIB,
+            transcendentals=0,
+        ),
+        name="combine",
+    )(routes.T, weights.T, *pieces)
+
+
+def finish_kernel(sum_ref, high_ref, low_ref, *refs):
+    pieces, out_ref = refs[:-1], refs[-1]
+    total = sum_ref[...]
+    for place, ref in enumerate(pieces):
+        rows = ref.shape[0]
+        for scales in (high_ref, low_ref):
+            total = total + dot(scales[:, place * rows : (place + 1) * rows], ref[...])
+    out_ref[...] = total.astype(BF)
+
+
+def finish(total, high, low, pieces):
+    return pl.pallas_call(
+        finish_kernel,
+        out_shape=jax.ShapeDtypeStruct(total.shape, BF),
+        in_specs=whole_specs(3 + len(pieces)),
+        out_specs=pl.BlockSpec(memory_space=pltpu.VMEM),
+        compiler_params=kernel_params(8),
+        cost_estimate=pl.CostEstimate(flops=16 * MIB, bytes_accessed=MIB, transcendentals=0),
+        name="finish",
+    )(total, high, low, *pieces)
+
+
+def attention_kernel(q_ref, k_ref, v_ref, rim_ref, sink_ref, freq_ref, out_ref, k_all, v_all):
+    rows, columns = q_ref.shape
+    heads = columns // HD
+    group = lax.axis_index("tp") * heads // (HEADS // KV)
+    half = HD // 2
+    lanes = k_ref.shape[1]
+    packed = freq_ref.shape[1] // half
+    lines = (WINDOW + rows) // packed
+    row = lax.broadcasted_iota(jnp.int32, (lines, packed * half), 0)
+    part = lax.broadcasted_iota(jnp.int32, (lines, packed * half), 1) // half
+    position = lax.axis_index("ep") * rows - WINDOW + part * lines + row
+    angles = position.astype(F32) * freq_ref[...]
+    tables = []
+    for table in (jnp.cos(angles), jnp.sin(angles)):
+        tables.append(jnp.concatenate([table[:, i * half : (i + 1) * half] for i in range(packed)], 0))
+
+    def rotated(value, start, count):
+        size = value.shape[1]
+        row = lax.broadcasted_iota(jnp.int32, (size, size), 0)
+        column = lax.broadcasted_iota(jnp.int32, (size, size), 1)
+        upper = lax.rem(column, HD) >= half
+        swap = jnp.where(upper & (row == column - half), 1.0, 0.0)
+        swap = jnp.where(jnp.logical_not(upper) & (row == column + half), -1.0, swap)
+        cosine, sine = [table[start : start + count, :] for table in tables]
+        copies = size // half
+        cosine, sine = jnp.concatenate([cosine] * copies, 1), jnp.concatenate([sine] * copies, 1)
+        return value.astype(F32) * cosine + dot(value, swap.astype(BF)) * sine
+
+    def grouped(value):
+        picked = value[:, :HD]
+        for index in range(1, KV):
+            picked = jnp.where(group == index, value[:, index * HD : (index + 1) * HD], picked)
+        return picked
+
+    k_all[:WINDOW, :] = grouped(rotated(rim_ref[:, :lanes], 0, WINDOW)).astype(BF)
+    k_all[WINDOW:, :] = grouped(rotated(k_ref[...], WINDOW, rows)).astype(BF)
+    v_all[:WINDOW, :] = grouped(rim_ref[:, lanes:].astype(F32)).astype(BF)
+    v_all[WINDOW:, :] = grouped(v_ref[...].astype(F32)).astype(BF)
+    query = (rotated(q_ref[...], WINDOW, rows).astype(BF).astype(F32) * HD**-0.5).astype(BF)
+    stacked = heads * WINDOW
+    line = lax.broadcasted_iota(jnp.int32, (stacked, 2 * WINDOW), 0)
+    key_at = lax.broadcasted_iota(jnp.int32, (stacked, 2 * WINDOW), 1)
+    distance = lax.rem(line, WINDOW) + WINDOW - key_at
+    near = (distance >= 0) & (distance < WINDOW)
+    inside = near & ((key_at >= WINDOW) | (lax.axis_index("ep") > 0))
+    head_of = lax.broadcasted_iota(jnp.int32, (stacked, 1), 0) // WINDOW
+    sink = jnp.full((stacked, 1), sink_ref[0], F32)
+    for head in range(1, heads):
+        sink = jnp.where(head_of == head, sink_ref[head], sink)
+    for block in range(rows // WINDOW):
+        start = block * WINDOW
+        band = pl.ds(start, 2 * WINDOW)
+        lines = [query[start : start + WINDOW, h * HD : (h + 1) * HD] for h in range(heads)]
+        scores = lax.dot_general(
+            jnp.concatenate(lines, 0), k_all[band, :], (((1,), (1,)), ((), ())), preferred_element_type=F32
+        )
+        scores = jnp.where(near if block else inside, scores, mask_value)
+        top = jnp.maximum(jnp.max(scores, axis=1, keepdims=True), sink)
+        spread = jnp.exp(scores - top)
+        total = jnp.sum(spread, axis=1, keepdims=True) + jnp.exp(sink - top)
+        mix = dot((spread * (1.0 / total)).astype(BF), v_all[band, :])
+        mixes = [mix[h * WINDOW : (h + 1) * WINDOW, :] for h in range(heads)]
+        out_ref[start : start + WINDOW, :] = jnp.concatenate(mixes, 1).astype(BF)
+
+
+def attention(queries, keys, values, rim, sink_logits):
+    rows, columns = queries.shape
+    half = HD // 2
+    packed = 128 // half
+    inv_freq = 10000.0 ** (-np.arange(half, dtype=np.float64) * (2.0 / HD))
+    inv_freq = np.tile(inv_freq.astype(np.float32)[None, :], (1, packed))
+    return pl.pallas_call(
+        attention_kernel,
+        out_shape=jax.ShapeDtypeStruct((rows, columns), BF),
+        in_specs=whole_specs(4) + [pl.BlockSpec(memory_space=pltpu.SMEM)] + whole_specs(1),
+        out_specs=pl.BlockSpec(memory_space=pltpu.VMEM),
+        scratch_shapes=[pltpu.VMEM((WINDOW + rows, HD), BF)] * 2,
+        compiler_params=kernel_params(12),
+        cost_estimate=pl.CostEstimate(
+            flops=16 * rows * columns * 2 * WINDOW, bytes_accessed=2 * MIB, transcendentals=0
+        ),
+        name="attention",
+    )(queries, keys, values, rim, sink_logits, jnp.asarray(inv_freq))
+
+
+def fold_kernel(second_ref, near_ref, out_ref):
+    width = out_ref.shape[1]
+    out_ref[...] = (second_ref[...].astype(F32) + near_ref[:, width:].astype(F32)).astype(BF)
+
+
+def fold(second, near):
+    return pl.pallas_call(
+        fold_kernel,
+        out_shape=jax.ShapeDtypeStruct(second.shape, BF),
+        in_specs=whole_specs(2),
+        out_specs=pl.BlockSpec(memory_space=pltpu.VMEM),
+        compiler_params=kernel_params(4),
+        cost_estimate=pl.CostEstimate(flops=MIB, bytes_accessed=MIB, transcendentals=0),
+        name="fold",
+    )(second, near)
+
+
+def local_planes(
+    queries,
+    keys,
+    values,
+    sink_logits,
+    out_weight,
+    expert_input,
+    norm_gain,
+    routes,
+    route_weights,
+    gate_weight,
+    up_weight,
+    down_weight,
+):
+    n_ep, n_tp = lax.axis_size("ep"), lax.axis_size("tp")
+    chips = n_ep // 2
+    token_rows, features = expert_input.shape
+    capacity = 2 * routes.shape[1] * token_rows // n_ep
+    width = features // n_tp
+
+    def in_plane(value, order):
+        pairs = []
+        for device in range(n_ep):
+            step = 1 + (device + order) % 2
+            pairs += [(device * n_tp + i, device * n_tp + (i ^ step)) for i in range(n_tp)]
+        return lax.ppermute(value, ("ep", "tp"), pairs)
+
+    def along(value, mask):
+        return lax.ppermute(value, "ep", [(i, i ^ mask) for i in range(n_ep)])
+
+    def gathered(value):
+        near = in_plane(value, 0)
+        return value, near, in_plane(value, 1), in_plane(near, 1)
+
+    def scattered(mine, second, far):
+        near = in_plane(far, 0)
+        summed = fold(second, near)
+        last = in_plane(summed, 1)
+        return settle(mine, near, last)
+
+    weights = (gate_weight, up_weight, down_weight)
+    steps = tuple(range(chips - 1, 0, -1))
+    sent = dispatch(expert_input, norm_gain, routes, queries, keys, values, capacity, chips, width)
+    sent, (mine, other, rim), local = sent[:-6], sent[-6:-3], sent[-3:]
+    rim = passed_along(rim, "ep", 1)
+    own = [mine, along(other, 1)]
+    arrived = {}
+    for step in steps:
+        pair = [along(sent[2 * (chips - 1 - step) + i], 2 * step) for i in range(2)]
+        arrived[step] = [pair[0], along(pair[1], 1)]
+    head_mix = attention(*local, rim, sink_logits)
+    parts = gathered(head_mix)
+    attn_out = project(parts, out_weight)
+    outcome = experts(own, weights, width, 4, fetch=True)
+    weights, outcome = outcome[:3], outcome[3:]
+    same, cross = scattered(*outcome)
+    pieces = {0: [same, along(cross, 1)]}
+    for step in steps:
+        rows = arrived[step]
+        if step > NEAR:
+            rows = join(*rows)
+            rows = gathered(rows)
+        outcome = experts(rows, weights, width, 4)
+        same, cross = scattered(*outcome)
+        cross = along(cross, 1)
+        pieces[step] = [along(same, 2 * step), along(cross, 2 * step)]
+    turns = steps + (0,)
+    early = [piece for step in turns[:-LATE] for piece in pieces[step]]
+    tail = [piece for step in turns[-LATE:] for piece in pieces[step]]
+    so_far = combine(routes, route_weights, turns, LATE, early)
+    expert_out = finish(*so_far, tail)
+    return (attn_out, expert_out)
+
+
+def local_of(mesh):
+    chips = mesh.shape["ep"] // 2
+    paired = mesh.shape["ep"] == 2 * chips and chips & (chips - 1) == 0
+    return local_planes if mesh.shape["tp"] == 4 and paired else local_general
+
+
 def solution(mesh):
     return jax.shard_map(
-        local,
+        local_of(mesh),
         mesh=mesh,
         in_specs=(
             P("ep", "tp"),

time: 218 us -> 130 us (0.60)
  waiting for transfers between devices: 121 us -> 50.5 us
  starting transfers between devices: 6.3 us -> 49.7 us
  blocking collectives: 32.8 us -> 0 us
  Pallas kernels: 0 us -> 28.8 us
  matrix products: 22.8 us -> 0 us
  between operations: 14.2 us -> 0.89 us
  local copies, waits for them, and re-layouts: 10.8 us -> 0.03 us
  other arithmetic: 10 us -> 0 us
    all_gather x2 -> x0, waiting for transfers between devices: 74.9 us -> none  [the longest x1 51.5 us: local(): portion = lax.all_gather(arrived, 'tp', axis=2, tiled=True)]
    ppermute x0 -> x37, waiting for transfers between devices: none -> 49.6 us  [the longest x20 36.9 us: along(): return lax.ppermute(value, 'ep', [(i, i ^ mask) for i in range(n_ep)])]
    ppermute x0 -> x37, starting transfers between devices: none -> 48.5 us  [the longest x20 24.6 us: along(): return lax.ppermute(value, 'ep', [(i, i ^ mask) for i in range(n_ep)])]
    reduce_scatter x1 -> x0, waiting for transfers between devices: 45.6 us -> none  [local(): lax.psum_scatter(lax.dot_general(down_local, hidden, (((0,), (1,)), ((),...]
    all_to_all x1 -> x0, blocking collectives: 32.8 us -> none  [local(): lax.all_to_all(outgoing, 'ep', split_axis=0, concat_axis=0, tiled=True)]
    pallas_call x0 -> x19, Pallas kernels: none -> 28.8 us  [the longest x4 17.2 us: experts(): pl.pallas_call(functools.partial(experts_kernel, split, fetch, blocks), o...]
    dot_general x6 -> x0, matrix products: 22.8 us -> none  [the longest x1 7.64 us: local(): up_acc = jnp.dot(flat_piece, up_local, preferred_element_type=jnp.float32)]
    gather x3 -> x0, local copies, waits for them, and re-layouts: 6.13 us -> none  [the longest x1 3.97 us: local(): jnp.take(own_columns, jnp.maximum(source_row, 0), axis=0)]
  transfers between devices with their start and end apart: 5 -> 38, of which waited for: 3 -> 11; matrix products, arithmetic and copies ran while one was open for 4% -> 0% of each run, Pallas kernels for 0% -> 19%
where the time goes in v1:
time: 130 us
  waiting for transfers between devices  50.5 us (39%)
  starting transfers between devices  49.7 us (38%)
  Pallas kernels  28.8 us (22%)
    ppermute x20, waiting for transfers between devices, along(): return lax.ppermute(value, 'ep', [(i, i ^ mask) for i in range(n_ep)])  36.9 us
    ppermute x20, starting transfers between devices, along(): return lax.ppermute(value, 'ep', [(i, i ^ mask) for i in range(n_ep)])  24.6 us
    ppermute x17, starting transfers between devices, in_plane(): return lax.ppermute(value, ('ep', 'tp'), pairs)  23.9 us
    pallas_call x4, Pallas kernels, experts(): pl.pallas_call(functools.partial(experts_kernel, split, fetch, blocks), o...  17.2 us
    ppermute x17, waiting for transfers between devices, in_plane(): return lax.ppermute(value, ('ep', 'tp'), pairs)  12.7 us
    pallas_call x1, Pallas kernels, attention(): pl.pallas_call(attention_kernel, out_shape=jax.ShapeDtypeStruct((rows, co...  3.69 us
    pallas_call x1, Pallas kernels, dispatch(): pl.pallas_call(functools.partial(dispatch_kernel, capacity, chips), out_s...  2.63 us
  transfers between devices with their start and end apart: 38, of which 11 were waited for; matrix products, arithmetic and copies ran while one was open for 0% of the time, Pallas kernels for 19%

profile of v1, /device:TPU:0, one launch (start us, length us, event | category | flops | bytes accessed | tf_op | source)
XLA Modules:
  0.0 129.9 jit_solution(4355874641001766544)
XLA Ops:
  0.6 2.6 %dispatch.1 = (bf16[128,512]{1,0:T(8,128)(2,1)S(1)}, bf16[128,512]{1,0:T(8,128)(2,1)S(1)}, bf16[128,512]{1,0:T(8,128)(2,1)S(1)}, bf16[128,512]{1,0:T(8,128)(2,1)...) custom-call(bf16[256,2048]{1,0:T(8,128)(2,1)} %x_hbm.1, ...), custom_call_target="tpu_custom_call" | custom-call | flops 536870912 | bytes 4194304 | tf_op jit(solution)/shard_map/dispatch/pallas_call | solution.py:271
  3.3 4.1 %collective-permute-start.17 = (bf16[128,512]{1,0:T(8,128)(2,1)S(1)}, bf16[128,512]{1,0:T(8,128)(2,1)S(1)}, u32[]{:S(2)}, u32[]{:S(2)}) collective-permute-start(bf16[128,512]{1,0:T(8,128)(2,1)S(1)} %get-tuple-element.57), channel_id=1, source_target_pairs={{0,16},{4,20},{8,24},{12,28},{16,0},{20,4},{24,8},{28,12},{1,17},{... | collective-permute-start | bytes 393224 | tf_op jit(solution)/shard_map/ppermute | solution.py:653
  7.6 9.8 %collective-permute-done.17 = bf16[128,512]{1,0:T(8,128)(2,1)S(1)} collective-permute-done((bf16[128,512]{1,0:T(8,128)(2,1)S(1)}, bf16[128,512]{1,0:T(8,128)(2,1)S(1)}, u32[]{:S(2)}, u32[]{:S(2)}) %collective-permute-start.17) | collective-permute-done | bytes 131104 | tf_op jit(solution)/shard_map/ppermute | solution.py:653
  17.4 2.8 %collective-permute-start.5 = (bf16[128,512]{1,0:T(8,128)(2,1)S(1)}, bf16[128,512]{1,0:T(8,128)(2,1)S(1)}, u32[]{:S(2)}, u32[]{:S(2)}) collective-permute-start(bf16[128,512]{1,0:T(8,128)(2,1)S(1)} %get-tuple-element.45), channel_id=1, source_target_pairs={{0,24},{4,28},{8,16},{12,20},{16,8},{20,12},{24,0},{28,4},{1,25},{... | collective-permute-start | bytes 393224 | tf_op jit(solution)/shard_map/ppermute | solution.py:653
  20.2 1.6 %collective-permute-start.19 = (bf16[256,512]{1,0:T(8,128)(2,1)S(1)}, bf16[256,512]{1,0:T(8,128)(2,1)S(1)}, u32[]{:S(2)}, u32[]{:S(2)}) collective-permute-start(bf16[256,512]{1,0:T(8,128)(2,1)S(1)} %join.3.refs_0_), channel_id=1, source_target_pairs={{0,1},{1,0},{2,3},{3,2},{4,6},{5,7},{6,4},{7,5},{8,9},{9,8},{10,11... | collective-permute-start | bytes 786440 | tf_op jit(solution)/shard_map/ppermute | solution.py:650
  21.7 2.8 %collective-permute-start.4 = (bf16[128,512]{1,0:T(8,128)(2,1)S(1)}, bf16[128,512]{1,0:T(8,128)(2,1)S(1)}, u32[]{:S(2)}, u32[]{:S(2)}) collective-permute-start(bf16[128,512]{1,0:T(8,128)(2,1)S(1)} %get-tuple-element.44), channel_id=1, source_target_pairs={{0,24},{4,28},{8,16},{12,20},{16,8},{20,12},{24,0},{28,4},{1,25},{... | collective-permute-start | bytes 393224 | tf_op jit(solution)/shard_map/ppermute | solution.py:653
  25.3 14.0 %collective-permute-done.4.top_ref = bf16[128,512]{1,0:T(8,128)(2,1)S(1)} collective-permute-done((bf16[128,512]{1,0:T(8,128)(2,1)S(1)}, bf16[128,512]{1,0:T(8,128)(2,1)S(1)}, u32[]{:S(2)}, u32[]{:S(2)}) %collective-permute-start.4) | collective-permute-done | bytes 131104 | tf_op jit(solution)/shard_map/ppermute | solution.py:653
  39.2 1.9 %collective-permute-start.20 = (bf16[256,512]{1,0:T(8,128)(2,1)S(1)}, bf16[256,512]{1,0:T(8,128)(2,1)S(1)}, u32[]{:S(2)}, u32[]{:S(2)}) collective-permute-start(bf16[256,512]{1,0:T(8,128)(2,1)S(1)} %join.3.refs_0_), channel_id=1, source_target_pairs={{0,2},{1,3},{2,0},{3,1},{4,5},{5,4},{6,7},{7,6},{8,10},{9,11},{10,... | collective-permute-start | bytes 786440 | tf_op jit(solution)/shard_map/ppermute | solution.py:650
  41.1 1.5 %collective-permute-start.7 = (bf16[256,512]{1,0:T(8,128)(2,1)S(1)}, bf16[256,512]{1,0:T(8,128)(2,1)S(1)}, u32[]{:S(2)}, u32[]{:S(2)}) collective-permute-start(bf16[256,512]{1,0:T(8,128)(2,1)S(1)} %join.2.refs_0_), channel_id=1, source_target_pairs={{0,1},{1,0},{2,3},{3,2},{4,6},{5,7},{6,4},{7,5},{8,9},{9,8},{10,11... | collective-permute-start | bytes 786440 | tf_op jit(solution)/shard_map/ppermute | solution.py:650
  43.2 6.4 %experts.4 = (bf16[1,2048,1024]{2,1,0:T(8,128)(2,1)S(1)}, bf16[1,2048,1024]{2,1,0:T(8,128)(2,1)S(1)}, bf16[1,1024,2048]{2,1,0:T(8,128)(2,1)S(1)}, bf16[256,512]{...) custom-call(bf16[128,2048]{1,0:T(8,128)(2,1)S(1)} %get-tuple-element.46.refs_0_, ...), custom_call_target="tpu_custom_call" | custom-call | flops 3221225472 | bytes 12582912 | tf_op jit(solution)/shard_map/experts/pallas_call | solution.py:360
  49.6 1.6 %collective-permute-start.8 = (bf16[256,512]{1,0:T(8,128)(2,1)S(1)}, bf16[256,512]{1,0:T(8,128)(2,1)S(1)}, u32[]{:S(2)}, u32[]{:S(2)}) collective-permute-start(bf16[256,512]{1,0:T(8,128)(2,1)S(1)} %join.2.refs_0_), channel_id=1, source_target_pairs={{0,2},{1,3},{2,0},{3,1},{4,5},{5,4},{6,7},{7,6},{8,10},{9,11},{10,... | collective-permute-start | bytes 786440 | tf_op jit(solution)/shard_map/ppermute | solution.py:650
  51.7 3.5 %experts.6 = (bf16[256,512]{1,0:T(8,128)(2,1)S(1)}, bf16[256,512]{1,0:T(8,128)(2,1)S(1)}, bf16[256,1024]{1,0:T(8,128)(2,1)S(1)}) custom-call(bf16[256,512]{1,0:T(8,128)(2,1)S(1)} %join.3.refs_0_, bf16[256,512]{1,0:T(8,128)(2,1)S(1)} %collective-permute-done.19.refs_1_, bf16[256,512]{1,0:T(8,128)(2,1)S(1)} %collective-permute-done.20.refs_2_, ...), custom_call_target="tpu_custom_call" | custom-call | flops 3221225472 | bytes 12582912 | tf_op jit(solution)/shard_map/experts/pallas_call | solution.py:360
  56.0 3.8 %collective-permute-done.9.refs_3_ = bf16[256,512]{1,0:T(8,128)(2,1)S(1)} collective-permute-done((bf16[256,512]{1,0:T(8,128)(2,1)S(1)}, bf16[256,512]{1,0:T(8,128)(2,1)S(1)}, u32[]{:S(2)}, u32[]{:S(2)}) %collective-permute-start.9) | collective-permute-done | bytes 262176 | tf_op jit(solution)/shard_map/ppermute | solution.py:650
  59.8 3.5 %experts.5 = (bf16[256,512]{1,0:T(8,128)(2,1)S(1)}, bf16[256,512]{1,0:T(8,128)(2,1)S(1)}, bf16[256,1024]{1,0:T(8,128)(2,1)S(1)}) custom-call(bf16[256,512]{1,0:T(8,128)(2,1)S(1)} %join.2.refs_0_, bf16[256,512]{1,0:T(8,128)(2,1)S(1)} %collective-permute-done.7.refs_1_, bf16[256,512]{1,0:T(8,128)(2,1)S(1)} %collective-permute-done.8.refs_2_, ...), custom_call_target="tpu_custom_call" | custom-call | flops 3221225472 | bytes 12582912 | tf_op jit(solution)/shard_map/experts/pallas_call | solution.py:360
  63.4 3.7 %experts.7 = (bf16[256,512]{1,0:T(8,128)(2,1)S(1)}, bf16[256,512]{1,0:T(8,128)(2,1)S(1)}, bf16[256,1024]{1,0:T(8,128)(2,1)S(1)}) custom-call(bf16[128,2048]{1,0:T(8,128)(2,1)S(1)} %collective-permute-done.27.refs_0_, bf16[128,2048]{1,0:T(8,128)(2,1)S(1)} %collective-permute-done.29.refs_1_, bf16[1,2048,1024]{2,1,0:T(8,128)(2,1)S(1)} %get-tuple-element.48.refs_4_.refs_2_, ...), custom_call_target="tpu_custom_call" | custom-call | flops 3221225472 | bytes 12582912 | tf_op jit(solution)/shard_map/experts/pallas_call | solution.py:360
  67.1 2.0 %collective-permute-start.30 = (bf16[256,1024]{1,0:T(8,128)(2,1)S(1)}, bf16[256,1024]{1,0:T(8,128)(2,1)S(1)}, u32[]{:S(2)}, u32[]{:S(2)}) collective-permute-start(bf16[256,1024]{1,0:T(8,128)(2,1)S(1)} %get-tuple-element.69), channel_id=1, source_target_pairs={{0,1},{1,0},{2,3},{3,2},{4,6},{5,7},{6,4},{7,5},{8,9},{9,8},{10,11... | collective-permute-start | bytes 1572872 | tf_op jit(solution)/shard_map/ppermute | solution.py:650
  71.4 3.7 %attention.1.refs_0_ = bf16[512,256]{1,0:T(8,128)(2,1)S(1)} custom-call(bf16[512,256]{1,0:T(8,128)(2,1)S(1)} %get-tuple-element.40.q_ref, bf16[512,128]{1,0:T(8,128)(2,1)S(1)} %get-tuple-element.41.k_ref, bf16[512,128]{1,0:T(8,128)(2,1)S(1)} %get-tuple-element.42.v_ref, bf16[128,256]{1,0:T(8,128)(2,1)S(1)} %collective-permute-done.rim_ref, f32[4]{0:T(128)S(1)} %copy-done.3, ...), custom_call_target="tpu_custom_call" | custom-call | flops 536870912 | bytes 2097152 | tf_op jit(solution)/shard_map/attention/pallas_call | solution.py:594
  75.1 2.0 %collective-permute-start.1 = (bf16[512,256]{1,0:T(8,128)(2,1)S(1)}, bf16[512,256]{1,0:T(8,128)(2,1)S(1)}, u32[]{:S(2)}, u32[]{:S(2)}) collective-permute-start(bf16[512,256]{1,0:T(8,128)(2,1)S(1)} %attention.1.refs_0_), channel_id=1, source_target_pairs={{0,1},{1,0},{2,3},{3,2},{4,6},{5,7},{6,4},{7,5},{8,9},{9,8},{10,11... | collective-permute-start | bytes 786440 | tf_op jit(solution)/shard_map/ppermute | solution.py:650
  77.2 2.5 %collective-permute-start.23 = (bf16[256,512]{1,0:T(8,128)(2,1)S(1)}, bf16[256,512]{1,0:T(8,128)(2,1)S(1)}, u32[]{:S(2)}, u32[]{:S(2)}) collective-permute-start(bf16[256,512]{1,0:T(8,128)(2,1)S(1)} %fold.5), channel_id=1, source_target_pairs={{0,2},{1,3},{2,0},{3,1},{4,5},{5,4},{6,7},{7,6},{8,10},{9,11},{10,... | collective-permute-start | bytes 786440 | tf_op jit(solution)/shard_map/ppermute | solution.py:650
  80.0 2.1 %collective-permute-start.31 = (bf16[256,512]{1,0:T(8,128)(2,1)S(1)}, bf16[256,512]{1,0:T(8,128)(2,1)S(1)}, u32[]{:S(2)}, u32[]{:S(2)}) collective-permute-start(bf16[256,512]{1,0:T(8,128)(2,1)S(1)} %fold.6), channel_id=1, source_target_pairs={{0,2},{1,3},{2,0},{3,1},{4,5},{5,4},{6,7},{7,6},{8,10},{9,11},{10,... | collective-permute-start | bytes 786440 | tf_op jit(solution)/shard_map/ppermute | solution.py:650
  82.1 7.7 %collective-permute-done.1.refs_1_ = bf16[512,256]{1,0:T(8,128)(2,1)S(1)} collective-permute-done((bf16[512,256]{1,0:T(8,128)(2,1)S(1)}, bf16[512,256]{1,0:T(8,128)(2,1)S(1)}, u32[]{:S(2)}, u32[]{:S(2)}) %collective-permute-start.1) | collective-permute-done | bytes 262176 | tf_op jit(solution)/shard_map/ppermute | solution.py:650
  89.8 4.6 %collective-permute-start.2 = (bf16[512,256]{1,0:T(8,128)(2,1)S(1)}, bf16[512,256]{1,0:T(8,128)(2,1)S(1)}, u32[]{:S(2)}, u32[]{:S(2)}) collective-permute-start(bf16[512,256]{1,0:T(8,128)(2,1)S(1)} %attention.1.refs_0_), channel_id=1, source_target_pairs={{0,2},{1,3},{2,0},{3,1},{4,5},{5,4},{6,7},{7,6},{8,10},{9,11},{10,... | collective-permute-start | bytes 786440 | tf_op jit(solution)/shard_map/ppermute | solution.py:650
  94.5 2.1 %collective-permute-start.36 = (bf16[256,512]{1,0:T(8,128)(2,1)S(1)}, bf16[256,512]{1,0:T(8,128)(2,1)S(1)}, u32[]{:S(2)}, u32[]{:S(2)}) collective-permute-start(bf16[256,512]{1,0:T(8,128)(2,1)S(1)} %fold.7), channel_id=1, source_target_pairs={{0,2},{1,3},{2,0},{3,1},{4,5},{5,4},{6,7},{7,6},{8,10},{9,11},{10,... | collective-permute-start | bytes 786440 | tf_op jit(solution)/shard_map/ppermute | solution.py:650
  98.7 4.8 %collective-permute-start.24 = (bf16[128,512]{1,0:T(8,128)(2,1)S(1)}, bf16[128,512]{1,0:T(8,128)(2,1)S(1)}, u32[]{:S(2)}, u32[]{:S(2)}) collective-permute-start(bf16[128,512]{1,0:T(8,128)(2,1)S(1)} %get-tuple-element.61), channel_id=1, source_target_pairs={{0,16},{4,20},{8,24},{12,28},{16,0},{20,4},{24,8},{28,12},{1,17},{... | collective-permute-start | bytes 393224 | tf_op jit(solution)/shard_map/ppermute | solution.py:653
  103.6 2.4 %collective-permute-start.13 = (bf16[128,512]{1,0:T(8,128)(2,1)S(1)}, bf16[128,512]{1,0:T(8,128)(2,1)S(1)}, u32[]{:S(2)}, u32[]{:S(2)}) collective-permute-start(bf16[128,512]{1,0:T(8,128)(2,1)S(1)} %get-tuple-element.54), channel_id=1, source_target_pairs={{0,24},{4,28},{8,16},{12,20},{16,8},{20,12},{24,0},{28,4},{1,25},{... | collective-permute-start | bytes 393224 | tf_op jit(solution)/shard_map/ppermute | solution.py:653
  106.0 3.2 %collective-permute-start.26 = (bf16[128,512]{1,0:T(8,128)(2,1)S(1)}, bf16[128,512]{1,0:T(8,128)(2,1)S(1)}, u32[]{:S(2)}, u32[]{:S(2)}) collective-permute-start(bf16[128,512]{1,0:T(8,128)(2,1)S(1)} %collective-permute-done.25), channel_id=1, source_target_pairs={{0,16},{4,20},{8,24},{12,28},{16,0},{20,4},{24,8},{28,12},{1,17},{... | collective-permute-start | bytes 393224 | tf_op jit(solution)/shard_map/ppermute | solution.py:653
  109.5 8.2 %collective-permute-done.24.refs_4_ = bf16[128,512]{1,0:T(8,128)(2,1)S(1)} collective-permute-done((bf16[128,512]{1,0:T(8,128)(2,1)S(1)}, bf16[128,512]{1,0:T(8,128)(2,1)S(1)}, u32[]{:S(2)}, u32[]{:S(2)}) %collective-permute-start.24) | collective-permute-done | bytes 131104 | tf_op jit(solution)/shard_map/ppermute | solution.py:653
  117.7 3.4 %collective-permute-start.32 = (bf16[128,512]{1,0:T(8,128)(2,1)S(1)}, bf16[128,512]{1,0:T(8,128)(2,1)S(1)}, u32[]{:S(2)}, u32[]{:S(2)}) collective-permute-start(bf16[128,512]{1,0:T(8,128)(2,1)S(1)} %get-tuple-element.71), channel_id=1, source_target_pairs={{0,8},{4,12},{8,0},{12,4},{16,24},{20,28},{24,16},{28,20},{1,9},{5... | collective-permute-start | bytes 393224 | tf_op jit(solution)/shard_map/ppermute | solution.py:653
  121.1 1.5 %project.1 = bf16[512,512]{1,0:T(8,128)(2,1)} custom-call(bf16[512,256]{1,0:T(8,128)(2,1)S(1)} %attention.1.refs_0_, bf16[512,256]{1,0:T(8,128)(2,1)S(1)} %collective-permute-done.1.refs_1_, bf16[512,256]{1,0:T(8,128)(2,1)S(1)} %collective-permute-done.2.refs_2_, bf16[512,256]{1,0:T(8,128)(2,1)S(1)} %collective-permute-done.3.refs_3_, ...), custom_call_target="tpu_custom_call" | custom-call | flops 536870912 | bytes 3145728 | tf_op jit(solution)/shard_map/project/pallas_call | solution.py:430
  123.4 1.7 %combine.1 = (f32[256,512]{1,0:T(8,128)S(1)}, bf16[256,512]{1,0:T(8,128)(2,1)S(1)}, bf16[256,512]{1,0:T(8,128)(2,1)S(1)}) custom-call(s32[2,256]{1,0:T(2,128)S(1)} %bitcast.4, f32[2,256]{1,0:T(2,128)S(1)} %bitcast.5, bf16[128,512]{1,0:T(8,128)(2,1)S(1)} %collective-permute-done.13.refs_2_, bf16[128,512]{1,0:T(8,128)(2,1)S(1)} %collective-permute-done.15.refs_3_, ...), custom_call_target="tpu_custom_call" | custom-call | flops 268435456 | bytes 2097152 | tf_op jit(solution)/shard_map/combine/pallas_call | solution.py:482
  125.8 2.7 %collective-permute-done.34.refs_1_ = bf16[128,512]{1,0:T(8,128)(2,1)S(1)} collective-permute-done((bf16[128,512]{1,0:T(8,128)(2,1)S(1)}, bf16[128,512]{1,0:T(8,128)(2,1)S(1)}, u32[]{:S(2)}, u32[]{:S(2)}) %collective-permute-start.34) | collective-permute-done | bytes 131104 | tf_op jit(solution)/shard_map/ppermute | solution.py:653
  128.5 1.4 %finish.1 = bf16[256,512]{1,0:T(8,128)(2,1)} custom-call(f32[256,512]{1,0:T(8,128)S(1)} %get-tuple-element.63.sum_ref, bf16[256,512]{1,0:T(8,128)(2,1)S(1)} %get-tuple-element.64.high_ref, bf16[256,512]{1,0:T(8,128)(2,1)S(1)} %get-tuple-element.65.low_ref, bf16[128,512]{1,0:T(8,128)(2,1)S(1)} %collective-permute-done.32.refs_0_, ...), custom_call_target="tpu_custom_call" | custom-call | flops 16777216 | bytes 1048576 | tf_op jit(solution)/shard_map/finish/pallas_call | solution.py:512
  (73 shorter events, 9.4 us)
Async XLA Ops:
  3.3 14.1 %collective-permute-start.17 = (bf16[128,512]{1,0:T(8,128)(2,1)S(1)}, bf16[128,512]{1,0:T(8,128)(2,1)S(1)}, u32[]{:S(2)}, u32[]{:S(2)}) collective-permute-start(bf16[128,512]{1,0:T(8,128)(2,1)S(1)} %get-tuple-element.57), channel_id=1, source_target_pairs={{0,16},{4,20},{8,24},{12,28},{16,0},{20,4},{24,8},{28,12},{1,17},{... | collective-permute-start | bytes 393224 | tf_op jit(solution)/shard_map/ppermute | solution.py:653
  7.4 33.7 %collective-permute-start.10 = (bf16[128,2048]{1,0:T(8,128)(2,1)S(1)}, bf16[128,2048]{1,0:T(8,128)(2,1)S(1)}, u32[]{:S(2)}, u32[]{:S(2)}) collective-permute-start(bf16[128,2048]{1,0:T(8,128)(2,1)S(1)} %get-tuple-element.47), channel_id=1, source_target_pairs={{0,4},{4,0},{8,12},{12,8},{16,20},{20,16},{24,28},{28,24},{1,5},{5... | collective-permute-start | bytes 1572872 | tf_op jit(solution)/shard_map/ppermute | solution.py:653
  7.4 12.7 %collective-permute-start.16 = (bf16[128,512]{1,0:T(8,128)(2,1)S(1)}, bf16[128,512]{1,0:T(8,128)(2,1)S(1)}, u32[]{:S(2)}, u32[]{:S(2)}) collective-permute-start(bf16[128,512]{1,0:T(8,128)(2,1)S(1)} %get-tuple-element.56), channel_id=1, source_target_pairs={{0,16},{4,20},{8,24},{12,28},{16,0},{20,4},{24,8},{28,12},{1,17},{... | collective-permute-start | bytes 393224 | tf_op jit(solution)/shard_map/ppermute | solution.py:653
  20.2 22.5 %collective-permute-start.19 = (bf16[256,512]{1,0:T(8,128)(2,1)S(1)}, bf16[256,512]{1,0:T(8,128)(2,1)S(1)}, u32[]{:S(2)}, u32[]{:S(2)}) collective-permute-start(bf16[256,512]{1,0:T(8,128)(2,1)S(1)} %join.3.refs_0_), channel_id=1, source_target_pairs={{0,1},{1,0},{2,3},{3,2},{4,6},{5,7},{6,4},{7,5},{8,9},{9,8},{10,11... | collective-permute-start | bytes 786440 | tf_op jit(solution)/shard_map/ppermute | solution.py:650
  21.7 27.8 %collective-permute-start.28 = (bf16[128,2048]{1,0:T(8,128)(2,1)S(1)}, bf16[128,2048]{1,0:T(8,128)(2,1)S(1)}, u32[]{:S(2)}, u32[]{:S(2)}) collective-permute-start(bf16[128,2048]{1,0:T(8,128)(2,1)S(1)} %get-tuple-element.67), channel_id=1, source_target_pairs={{0,8},{4,12},{8,0},{12,4},{16,24},{20,28},{24,16},{28,20},{1,9},{5... | collective-permute-start | bytes 1572872 | tf_op jit(solution)/shard_map/ppermute | solution.py:653
  21.7 17.5 %collective-permute-start.4 = (bf16[128,512]{1,0:T(8,128)(2,1)S(1)}, bf16[128,512]{1,0:T(8,128)(2,1)S(1)}, u32[]{:S(2)}, u32[]{:S(2)}) collective-permute-start(bf16[128,512]{1,0:T(8,128)(2,1)S(1)} %get-tuple-element.44), channel_id=1, source_target_pairs={{0,24},{4,28},{8,16},{12,20},{16,8},{20,12},{24,0},{28,4},{1,25},{... | collective-permute-start | bytes 393224 | tf_op jit(solution)/shard_map/ppermute | solution.py:653
  25.3 14.0 %collective-permute-start.6 = (bf16[128,512]{1,0:T(8,128)(2,1)S(1)}, bf16[128,512]{1,0:T(8,128)(2,1)S(1)}, u32[]{:S(2)}, u32[]{:S(2)}) collective-permute-start(bf16[128,512]{1,0:T(8,128)(2,1)S(1)} %collective-permute-done.5), channel_id=1, source_target_pairs={{0,4},{4,0},{8,12},{12,8},{16,20},{20,16},{24,28},{28,24},{1,5},{5... | collective-permute-start | bytes 393224 | tf_op jit(solution)/shard_map/ppermute | solution.py:653
  39.2 24.2 %collective-permute-start.27 = (bf16[128,2048]{1,0:T(8,128)(2,1)S(1)}, bf16[128,2048]{1,0:T(8,128)(2,1)S(1)}, u32[]{:S(2)}, u32[]{:S(2)}) collective-permute-start(bf16[128,2048]{1,0:T(8,128)(2,1)S(1)} %get-tuple-element.66), channel_id=1, source_target_pairs={{0,8},{4,12},{8,0},{12,4},{16,24},{20,28},{24,16},{28,20},{1,9},{5... | collective-permute-start | bytes 1572872 | tf_op jit(solution)/shard_map/ppermute | solution.py:653
  39.2 11.9 %collective-permute-start.20 = (bf16[256,512]{1,0:T(8,128)(2,1)S(1)}, bf16[256,512]{1,0:T(8,128)(2,1)S(1)}, u32[]{:S(2)}, u32[]{:S(2)}) collective-permute-start(bf16[256,512]{1,0:T(8,128)(2,1)S(1)} %join.3.refs_0_), channel_id=1, source_target_pairs={{0,2},{1,3},{2,0},{3,1},{4,5},{5,4},{6,7},{7,6},{8,10},{9,11},{10,... | collective-permute-start | bytes 786440 | tf_op jit(solution)/shard_map/ppermute | solution.py:650
  41.1 10.1 %collective-permute-start.7 = (bf16[256,512]{1,0:T(8,128)(2,1)S(1)}, bf16[256,512]{1,0:T(8,128)(2,1)S(1)}, u32[]{:S(2)}, u32[]{:S(2)}) collective-permute-start(bf16[256,512]{1,0:T(8,128)(2,1)S(1)} %join.2.refs_0_), channel_id=1, source_target_pairs={{0,1},{1,0},{2,3},{3,2},{4,6},{5,7},{6,4},{7,5},{8,9},{9,8},{10,11... | collective-permute-start | bytes 786440 | tf_op jit(solution)/shard_map/ppermute | solution.py:650
  42.7 9.1 %collective-permute-start.21 = (bf16[256,512]{1,0:T(8,128)(2,1)S(1)}, bf16[256,512]{1,0:T(8,128)(2,1)S(1)}, u32[]{:S(2)}, u32[]{:S(2)}) collective-permute-start(bf16[256,512]{1,0:T(8,128)(2,1)S(1)} %collective-permute-done.19.refs_1_), channel_id=1, source_target_pairs={{0,2},{1,3},{2,0},{3,1},{4,5},{5,4},{6,7},{7,6},{8,10},{9,11},{10,... | collective-permute-start | bytes 786440 | tf_op jit(solution)/shard_map/ppermute | solution.py:650
  51.2 12.3 %collective-permute-start.29 = (bf16[128,2048]{1,0:T(8,128)(2,1)S(1)}, bf16[128,2048]{1,0:T(8,128)(2,1)S(1)}, u32[]{:S(2)}, u32[]{:S(2)}) collective-permute-start(bf16[128,2048]{1,0:T(8,128)(2,1)S(1)} %collective-permute-done.28), channel_id=1, source_target_pairs={{0,4},{4,0},{8,12},{12,8},{16,20},{20,16},{24,28},{28,24},{1,5},{5... | collective-permute-start | bytes 1572872 | tf_op jit(solution)/shard_map/ppermute | solution.py:653
  51.2 8.6 %collective-permute-start.9 = (bf16[256,512]{1,0:T(8,128)(2,1)S(1)}, bf16[256,512]{1,0:T(8,128)(2,1)S(1)}, u32[]{:S(2)}, u32[]{:S(2)}) collective-permute-start(bf16[256,512]{1,0:T(8,128)(2,1)S(1)} %collective-permute-done.7.refs_1_), channel_id=1, source_target_pairs={{0,2},{1,3},{2,0},{3,1},{4,5},{5,4},{6,7},{7,6},{8,10},{9,11},{10,... | collective-permute-start | bytes 786440 | tf_op jit(solution)/shard_map/ppermute | solution.py:650
  55.3 21.9 %collective-permute-start.22 = (bf16[256,1024]{1,0:T(8,128)(2,1)S(1)}, bf16[256,1024]{1,0:T(8,128)(2,1)S(1)}, u32[]{:S(2)}, u32[]{:S(2)}) collective-permute-start(bf16[256,1024]{1,0:T(8,128)(2,1)S(1)} %get-tuple-element.59), channel_id=1, source_target_pairs={{0,1},{1,0},{2,3},{3,2},{4,6},{5,7},{6,4},{7,5},{8,9},{9,8},{10,11... | collective-permute-start | bytes 1572872 | tf_op jit(solution)/shard_map/ppermute | solution.py:650
  63.3 16.4 %collective-permute-start.11 = (bf16[256,1024]{1,0:T(8,128)(2,1)S(1)}, bf16[256,1024]{1,0:T(8,128)(2,1)S(1)}, u32[]{:S(2)}, u32[]{:S(2)}) collective-permute-start(bf16[256,1024]{1,0:T(8,128)(2,1)S(1)} %get-tuple-element.52), channel_id=1, source_target_pairs={{0,1},{1,0},{2,3},{3,2},{4,6},{5,7},{6,4},{7,5},{8,9},{9,8},{10,11... | collective-permute-start | bytes 1572872 | tf_op jit(solution)/shard_map/ppermute | solution.py:650
  67.1 12.8 %collective-permute-start.30 = (bf16[256,1024]{1,0:T(8,128)(2,1)S(1)}, bf16[256,1024]{1,0:T(8,128)(2,1)S(1)}, u32[]{:S(2)}, u32[]{:S(2)}) collective-permute-start(bf16[256,1024]{1,0:T(8,128)(2,1)S(1)} %get-tuple-element.69), channel_id=1, source_target_pairs={{0,1},{1,0},{2,3},{3,2},{4,6},{5,7},{6,4},{7,5},{8,9},{9,8},{10,11... | collective-permute-start | bytes 1572872 | tf_op jit(solution)/shard_map/ppermute | solution.py:650
  69.2 25.2 %collective-permute-start.35 = (bf16[256,1024]{1,0:T(8,128)(2,1)S(1)}, bf16[256,1024]{1,0:T(8,128)(2,1)S(1)}, u32[]{:S(2)}, u32[]{:S(2)}) collective-permute-start(bf16[256,1024]{1,0:T(8,128)(2,1)S(1)} %get-tuple-element.74), channel_id=1, source_target_pairs={{0,1},{1,0},{2,3},{3,2},{4,6},{5,7},{6,4},{7,5},{8,9},{9,8},{10,11... | collective-permute-start | bytes 1572872 | tf_op jit(solution)/shard_map/ppermute | solution.py:650
  75.1 14.6 %collective-permute-start.1 = (bf16[512,256]{1,0:T(8,128)(2,1)S(1)}, bf16[512,256]{1,0:T(8,128)(2,1)S(1)}, u32[]{:S(2)}, u32[]{:S(2)}) collective-permute-start(bf16[512,256]{1,0:T(8,128)(2,1)S(1)} %attention.1.refs_0_), channel_id=1, source_target_pairs={{0,1},{1,0},{2,3},{3,2},{4,6},{5,7},{6,4},{7,5},{8,9},{9,8},{10,11... | collective-permute-start | bytes 786440 | tf_op jit(solution)/shard_map/ppermute | solution.py:650
  77.2 17.3 %collective-permute-start.23 = (bf16[256,512]{1,0:T(8,128)(2,1)S(1)}, bf16[256,512]{1,0:T(8,128)(2,1)S(1)}, u32[]{:S(2)}, u32[]{:S(2)}) collective-permute-start(bf16[256,512]{1,0:T(8,128)(2,1)S(1)} %fold.5), channel_id=1, source_target_pairs={{0,2},{1,3},{2,0},{3,1},{4,5},{5,4},{6,7},{7,6},{8,10},{9,11},{10,... | collective-permute-start | bytes 786440 | tf_op jit(solution)/shard_map/ppermute | solution.py:650
  79.8 16.8 %collective-permute-start.12 = (bf16[256,512]{1,0:T(8,128)(2,1)S(1)}, bf16[256,512]{1,0:T(8,128)(2,1)S(1)}, u32[]{:S(2)}, u32[]{:S(2)}) collective-permute-start(bf16[256,512]{1,0:T(8,128)(2,1)S(1)} %fold.4), channel_id=1, source_target_pairs={{0,2},{1,3},{2,0},{3,1},{4,5},{5,4},{6,7},{7,6},{8,10},{9,11},{10,... | collective-permute-start | bytes 786440 | tf_op jit(solution)/shard_map/ppermute | solution.py:650
  80.0 16.8 %collective-permute-start.31 = (bf16[256,512]{1,0:T(8,128)(2,1)S(1)}, bf16[256,512]{1,0:T(8,128)(2,1)S(1)}, u32[]{:S(2)}, u32[]{:S(2)}) collective-permute-start(bf16[256,512]{1,0:T(8,128)(2,1)S(1)} %fold.6), channel_id=1, source_target_pairs={{0,2},{1,3},{2,0},{3,1},{4,5},{5,4},{6,7},{7,6},{8,10},{9,11},{10,... | collective-permute-start | bytes 786440 | tf_op jit(solution)/shard_map/ppermute | solution.py:650
  89.8 9.0 %collective-permute-start.2 = (bf16[512,256]{1,0:T(8,128)(2,1)S(1)}, bf16[512,256]{1,0:T(8,128)(2,1)S(1)}, u32[]{:S(2)}, u32[]{:S(2)}) collective-permute-start(bf16[512,256]{1,0:T(8,128)(2,1)S(1)} %attention.1.refs_0_), channel_id=1, source_target_pairs={{0,2},{1,3},{2,0},{3,1},{4,5},{5,4},{6,7},{7,6},{8,10},{9,11},{10,... | collective-permute-start | bytes 786440 | tf_op jit(solution)/shard_map/ppermute | solution.py:650
  94.4 9.2 %collective-permute-start.3 = (bf16[512,256]{1,0:T(8,128)(2,1)S(1)}, bf16[512,256]{1,0:T(8,128)(2,1)S(1)}, u32[]{:S(2)}, u32[]{:S(2)}) collective-permute-start(bf16[512,256]{1,0:T(8,128)(2,1)S(1)} %collective-permute-done.1.refs_1_), channel_id=1, source_target_pairs={{0,2},{1,3},{2,0},{3,1},{4,5},{5,4},{6,7},{7,6},{8,10},{9,11},{10,... | collective-permute-start | bytes 786440 | tf_op jit(solution)/shard_map/ppermute | solution.py:650
  94.5 11.5 %collective-permute-start.36 = (bf16[256,512]{1,0:T(8,128)(2,1)S(1)}, bf16[256,512]{1,0:T(8,128)(2,1)S(1)}, u32[]{:S(2)}, u32[]{:S(2)}) collective-permute-start(bf16[256,512]{1,0:T(8,128)(2,1)S(1)} %fold.7), channel_id=1, source_target_pairs={{0,2},{1,3},{2,0},{3,1},{4,5},{5,4},{6,7},{7,6},{8,10},{9,11},{10,... | collective-permute-start | bytes 786440 | tf_op jit(solution)/shard_map/ppermute | solution.py:650
  96.7 9.3 %collective-permute-start.25 = (bf16[128,512]{1,0:T(8,128)(2,1)S(1)}, bf16[128,512]{1,0:T(8,128)(2,1)S(1)}, u32[]{:S(2)}, u32[]{:S(2)}) collective-permute-start(bf16[128,512]{1,0:T(8,128)(2,1)S(1)} %get-tuple-element.62), channel_id=1, source_target_pairs={{0,4},{4,0},{8,12},{12,8},{16,20},{20,16},{24,28},{28,24},{1,5},{5... | collective-permute-start | bytes 393224 | tf_op jit(solution)/shard_map/ppermute | solution.py:653
  96.9 12.3 %collective-permute-start.14 = (bf16[128,512]{1,0:T(8,128)(2,1)S(1)}, bf16[128,512]{1,0:T(8,128)(2,1)S(1)}, u32[]{:S(2)}, u32[]{:S(2)}) collective-permute-start(bf16[128,512]{1,0:T(8,128)(2,1)S(1)} %get-tuple-element.55), channel_id=1, source_target_pairs={{0,4},{4,0},{8,12},{12,8},{16,20},{20,16},{24,28},{28,24},{1,5},{5... | collective-permute-start | bytes 393224 | tf_op jit(solution)/shard_map/ppermute | solution.py:653
  98.7 19.0 %collective-permute-start.24 = (bf16[128,512]{1,0:T(8,128)(2,1)S(1)}, bf16[128,512]{1,0:T(8,128)(2,1)S(1)}, u32[]{:S(2)}, u32[]{:S(2)}) collective-permute-start(bf16[128,512]{1,0:T(8,128)(2,1)S(1)} %get-tuple-element.61), channel_id=1, source_target_pairs={{0,16},{4,20},{8,24},{12,28},{16,0},{20,4},{24,8},{28,12},{1,17},{... | collective-permute-start | bytes 393224 | tf_op jit(solution)/shard_map/ppermute | solution.py:653
  103.6 14.2 %collective-permute-start.13 = (bf16[128,512]{1,0:T(8,128)(2,1)S(1)}, bf16[128,512]{1,0:T(8,128)(2,1)S(1)}, u32[]{:S(2)}, u32[]{:S(2)}) collective-permute-start(bf16[128,512]{1,0:T(8,128)(2,1)S(1)} %get-tuple-element.54), channel_id=1, source_target_pairs={{0,24},{4,28},{8,16},{12,20},{16,8},{20,12},{24,0},{28,4},{1,25},{... | collective-permute-start | bytes 393224 | tf_op jit(solution)/shard_map/ppermute | solution.py:653
  106.0 15.1 %collective-permute-start.33 = (bf16[128,512]{1,0:T(8,128)(2,1)S(1)}, bf16[128,512]{1,0:T(8,128)(2,1)S(1)}, u32[]{:S(2)}, u32[]{:S(2)}) collective-permute-start(bf16[128,512]{1,0:T(8,128)(2,1)S(1)} %get-tuple-element.72), channel_id=1, source_target_pairs={{0,4},{4,0},{8,12},{12,8},{16,20},{20,16},{24,28},{28,24},{1,5},{5... | collective-permute-start | bytes 393224 | tf_op jit(solution)/shard_map/ppermute | solution.py:653
  106.0 17.3 %collective-permute-start.26 = (bf16[128,512]{1,0:T(8,128)(2,1)S(1)}, bf16[128,512]{1,0:T(8,128)(2,1)S(1)}, u32[]{:S(2)}, u32[]{:S(2)}) collective-permute-start(bf16[128,512]{1,0:T(8,128)(2,1)S(1)} %collective-permute-done.25), channel_id=1, source_target_pairs={{0,16},{4,20},{8,24},{12,28},{16,0},{20,4},{24,8},{28,12},{1,17},{... | collective-permute-start | bytes 393224 | tf_op jit(solution)/shard_map/ppermute | solution.py:653
  109.2 14.2 %collective-permute-start.15 = (bf16[128,512]{1,0:T(8,128)(2,1)S(1)}, bf16[128,512]{1,0:T(8,128)(2,1)S(1)}, u32[]{:S(2)}, u32[]{:S(2)}) collective-permute-start(bf16[128,512]{1,0:T(8,128)(2,1)S(1)} %collective-permute-done.14), channel_id=1, source_target_pairs={{0,24},{4,28},{8,16},{12,20},{16,8},{20,12},{24,0},{28,4},{1,25},{... | collective-permute-start | bytes 393224 | tf_op jit(solution)/shard_map/ppermute | solution.py:653
  117.7 8.1 %collective-permute-start.32 = (bf16[128,512]{1,0:T(8,128)(2,1)S(1)}, bf16[128,512]{1,0:T(8,128)(2,1)S(1)}, u32[]{:S(2)}, u32[]{:S(2)}) collective-permute-start(bf16[128,512]{1,0:T(8,128)(2,1)S(1)} %get-tuple-element.71), channel_id=1, source_target_pairs={{0,8},{4,12},{8,0},{12,4},{16,24},{20,28},{24,16},{28,20},{1,9},{5... | collective-permute-start | bytes 393224 | tf_op jit(solution)/shard_map/ppermute | solution.py:653
  (11 other events, 180.9 us)

commit v2 on v1

--- a/solution.py
+++ b/solution.py
@@ -294,15 +294,15 @@
     rows_in = refs[:count]
     x, hidden = refs[-2:]
     if not fetch:
-        gate, up, down, mine_ref, second_ref, far_ref = refs[count:-2]
+        gate, up, down, *outs = refs[count:-2]
     else:
-        gate_hbm, up_hbm, down_hbm, gate, up, down, mine_ref, second_ref, far_ref, arrival = refs[count:-2]
+        gate_hbm, up_hbm, down_hbm, gate, up, down, *outs, arrival = refs[count:-2]
     here = lax.axis_index("tp")
     first, second = axes_here()
-    width = mine_ref.shape[1]
+    width = outs[0].shape[1]
     block = hidden.shape[1] // blocks
     parts = [pl.ds(step * block, block) for step in range(blocks)]
-    quarters = [quarter(index, width) for index in (here ^ first, here ^ 3, here ^ second, here)]
+    quarters = [quarter(index, width) for index in (here ^ 3, here ^ first, here ^ second, here)]
     copies = []
     if fetch:
         for place, part in enumerate(parts):
@@ -334,22 +334,14 @@
     for place, part in enumerate(quarters):
         for copy in copies[2 * blocks + place : 2 * blocks + place + 1]:
             copy.wait()
-        product = dot(hidden[...], down[0, :, part]).astype(BF)
-        if place < 2:
-            far_ref[:, place * width : (place + 1) * width] = product
-        else:
-            (second_ref if place == 2 else mine_ref)[...] = product
+        outs[3 - place][...] = dot(hidden[...], down[0, :, part]).astype(BF)
 
 
 def experts(rows_in, weights, width, blocks, fetch=False):
     split = len(rows_in) == 4
     rows = rows_in[0].shape[0] if split else 2 * rows_in[0].shape[0]
     _, features, hidden = weights[0].shape
-    out_shape = [
-        jax.ShapeDtypeStruct((rows, width), BF),
-        jax.ShapeDtypeStruct((rows, width), BF),
-        jax.ShapeDtypeStruct((rows, 2 * width), BF),
-    ]
+    out_shape = [jax.ShapeDtypeStruct((rows, width), BF)] * 4
     scratch = [pltpu.VMEM((rows, features), BF), pltpu.VMEM((rows, hidden), BF)]
     weight_specs = whole_specs(3)
     if fetch:
@@ -393,10 +385,10 @@
 
 
 def settle_kernel(mine_ref, near_ref, last_ref, same_ref, cross_ref):
-    rows, width = same_ref.shape
+    rows, _ = same_ref.shape
     for out_ref, start in ((same_ref, 0), (cross_ref, rows)):
         part = pl.ds(start, rows)
-        total = mine_ref[part, :].astype(F32) + near_ref[part, :width].astype(F32)
+        total = mine_ref[part, :].astype(F32) + near_ref[part, :].astype(F32)
         out_ref[...] = (total + last_ref[part, :].astype(F32)).astype(BF)
 
 
@@ -606,8 +598,7 @@
 
 
 def fold_kernel(second_ref, near_ref, out_ref):
-    width = out_ref.shape[1]
-    out_ref[...] = (second_ref[...].astype(F32) + near_ref[:, width:].astype(F32)).astype(BF)
+    out_ref[...] = (second_ref[...].astype(F32) + near_ref[...].astype(F32)).astype(BF)
 
 
 def fold(second, near):
@@ -656,10 +647,10 @@
         near = in_plane(value, 0)
         return value, near, in_plane(value, 1), in_plane(near, 1)
 
-    def scattered(mine, second, far):
-        near = in_plane(far, 0)
-        summed = fold(second, near)
-        last = in_plane(summed, 1)
+    def scattered(mine, second, first, both):
+        near = in_plane(both, 0)
+        last = in_plane(fold(second, near), 1)
+        near = in_plane(first, 0)
         return settle(mine, near, last)
 
     weights = (gate_weight, up_weight, down_weight)
@@ -670,8 +661,8 @@
     own = [mine, along(other, 1)]
     arrived = {}
     for step in steps:
-        pair = [along(sent[2 * (chips - 1 - step) + i], 2 * step) for i in range(2)]
-        arrived[step] = [pair[0], along(pair[1], 1)]
+        rows = sent[2 * (chips - 1 - step) :]
+        arrived[step] = [along(rows[i], 2 * step + i) for i in range(2)]
     head_mix = attention(*local, rim, sink_logits)
     parts = gathered(head_mix)
     attn_out = project(parts, out_weight)
@@ -686,8 +677,7 @@
             rows = gathered(rows)
         outcome = experts(rows, weights, width, 4)
         same, cross = scattered(*outcome)
-        cross = along(cross, 1)
-        pieces[step] = [along(same, 2 * step), along(cross, 2 * step)]
+        pieces[step] = [along(same, 2 * step), along(cross, 2 * step + 1)]
     turns = steps + (0,)
     early = [piece for step in turns[:-LATE] for piece in pieces[step]]
     tail = [piece for step in turns[-LATE:] for piece in pieces[step]]

time: 130 us -> 138 us (1.062)
  waiting for transfers between devices: 50.5 us -> 57.2 us
    ppermute x17 -> x21, waiting for transfers between devices: 12.7 us -> 26.1 us  [in_plane(): return lax.ppermute(value, ('ep', 'tp'), pairs)]
    ppermute x20 -> x14, waiting for transfers between devices: 36.9 us -> 31.1 us  [along(): return lax.ppermute(value, 'ep', [(i, i ^ mask) for i in range(n_ep)])]
    ppermute x20 -> x14, starting transfers between devices: 24.6 us -> 22.7 us  [along(): return lax.ppermute(value, 'ep', [(i, i ^ mask) for i in range(n_ep)])]
    ppermute x17 -> x21, starting transfers between devices: 23.9 us -> 24.9 us  [in_plane(): return lax.ppermute(value, ('ep', 'tp'), pairs)]
  transfers between devices with their start and end apart: 38 -> 36, of which waited for: 11 -> 12; matrix products, arithmetic and copies ran while one was open for 0% -> 0% of each run, Pallas kernels for 19% -> 18%
where the time goes in v2:
time: 138 us
  waiting for transfers between devices  57.2 us (41%)
  starting transfers between devices  49.5 us (36%)
  Pallas kernels  28.7 us (21%)
    ppermute x14, waiting for transfers between devices, along(): return lax.ppermute(value, 'ep', [(i, i ^ mask) for i in range(n_ep)])  31.1 us
    ppermute x21, waiting for transfers between devices, in_plane(): return lax.ppermute(value, ('ep', 'tp'), pairs)  26.1 us
    ppermute x21, starting transfers between devices, in_plane(): return lax.ppermute(value, ('ep', 'tp'), pairs)  24.9 us
    ppermute x14, starting transfers between devices, along(): return lax.ppermute(value, 'ep', [(i, i ^ mask) for i in range(n_ep)])  22.7 us
    pallas_call x4, Pallas kernels, experts(): pl.pallas_call(functools.partial(experts_kernel, split, fetch, blocks), o...  17.1 us
    pallas_call x1, Pallas kernels, attention(): pl.pallas_call(attention_kernel, out_shape=jax.ShapeDtypeStruct((rows, co...  3.69 us
  transfers between devices with their start and end apart: 36, of which 12 were waited for; matrix products, arithmetic and copies ran while one was open for 0% of the time, Pallas kernels for 18%

profile of v2, /device:TPU:0, one launch (start us, length us, event | category | flops | bytes accessed | tf_op | source)
XLA Modules:
  0.0 137.8 jit_solution(3236979295126558142)
XLA Ops:
  0.6 2.6 %dispatch.1 = (bf16[128,512]{1,0:T(8,128)(2,1)S(1)}, bf16[128,512]{1,0:T(8,128)(2,1)S(1)}, bf16[128,512]{1,0:T(8,128)(2,1)S(1)}, bf16[128,512]{1,0:T(8,128)(2,1)...) custom-call(bf16[256,2048]{1,0:T(8,128)(2,1)} %x_hbm.1, ...), custom_call_target="tpu_custom_call" | custom-call | flops 536870912 | bytes 4194304 | tf_op jit(solution)/shard_map/dispatch/pallas_call | solution.py:271
  3.8 1.9 %collective-permute-start = (bf16[128,256]{1,0:T(8,128)(2,1)S(1)}, bf16[128,256]{1,0:T(8,128)(2,1)S(1)}, u32[]{:S(2)}, u32[]{:S(2)}) collective-permute-start(bf16[128,256]{1,0:T(8,128)(2,1)S(1)} %get-tuple-element.47), channel_id=1, source_target_pairs={{0,4},{4,8},{8,12},{12,16},{16,20},{20,24},{24,28},{1,5},{5,9},{9,... | collective-permute-start | bytes 196616 | tf_op jit(solution)/shard_map/ppermute | solution.py:25
  5.8 4.1 %collective-permute-start.15 = (bf16[128,512]{1,0:T(8,128)(2,1)S(1)}, bf16[128,512]{1,0:T(8,128)(2,1)S(1)}, u32[]{:S(2)}, u32[]{:S(2)}) collective-permute-start(bf16[128,512]{1,0:T(8,128)(2,1)S(1)} %get-tuple-element.61), channel_id=1, source_target_pairs={{0,16},{4,20},{8,24},{12,28},{16,0},{20,4},{24,8},{28,12},{1,17},{... | collective-permute-start | bytes 393224 | tf_op jit(solution)/shard_map/ppermute | solution.py:644
  10.8 1.6 %collective-permute-start.25 = (bf16[128,2048]{1,0:T(8,128)(2,1)S(1)}, bf16[128,2048]{1,0:T(8,128)(2,1)S(1)}, u32[]{:S(2)}, u32[]{:S(2)}) collective-permute-start(bf16[128,2048]{1,0:T(8,128)(2,1)S(1)} %get-tuple-element.72), channel_id=1, source_target_pairs={{0,8},{4,12},{8,0},{12,4},{16,24},{20,28},{24,16},{28,20},{1,9},{5... | collective-permute-start | bytes 1572872 | tf_op jit(solution)/shard_map/ppermute | solution.py:644
  12.3 7.1 %collective-permute-done.15.top_ref = bf16[128,512]{1,0:T(8,128)(2,1)S(1)} collective-permute-done((bf16[128,512]{1,0:T(8,128)(2,1)S(1)}, bf16[128,512]{1,0:T(8,128)(2,1)S(1)}, u32[]{:S(2)}, u32[]{:S(2)}) %collective-permute-start.15) | collective-permute-done | bytes 131104 | tf_op jit(solution)/shard_map/ppermute | solution.py:644
  19.4 4.5 %collective-permute-start.4 = (bf16[128,512]{1,0:T(8,128)(2,1)S(1)}, bf16[128,512]{1,0:T(8,128)(2,1)S(1)}, u32[]{:S(2)}, u32[]{:S(2)}) collective-permute-start(bf16[128,512]{1,0:T(8,128)(2,1)S(1)} %get-tuple-element.48), channel_id=1, source_target_pairs={{0,24},{4,28},{8,16},{12,20},{16,8},{20,12},{24,0},{28,4},{1,25},{... | collective-permute-start | bytes 393224 | tf_op jit(solution)/shard_map/ppermute | solution.py:644
  23.9 2.2 %collective-permute-start.5 = (bf16[128,512]{1,0:T(8,128)(2,1)S(1)}, bf16[128,512]{1,0:T(8,128)(2,1)S(1)}, u32[]{:S(2)}, u32[]{:S(2)}) collective-permute-start(bf16[128,512]{1,0:T(8,128)(2,1)S(1)} %get-tuple-element.49), channel_id=1, source_target_pairs={{0,28},{4,24},{8,20},{12,16},{16,12},{20,8},{24,4},{28,0},{1,29},{... | collective-permute-start | bytes 393224 | tf_op jit(solution)/shard_map/ppermute | solution.py:644
  27.4 3.7 %attention.1.refs_0_ = bf16[512,256]{1,0:T(8,128)(2,1)S(1)} custom-call(bf16[512,256]{1,0:T(8,128)(2,1)S(1)} %get-tuple-element.44.q_ref, bf16[512,128]{1,0:T(8,128)(2,1)S(1)} %get-tuple-element.45.k_ref, bf16[512,128]{1,0:T(8,128)(2,1)S(1)} %get-tuple-element.46.v_ref, bf16[128,256]{1,0:T(8,128)(2,1)S(1)} %collective-permute-done.rim_ref, f32[4]{0:T(128)S(1)} %copy-done.3, ...), custom_call_target="tpu_custom_call" | custom-call | flops 536870912 | bytes 2097152 | tf_op jit(solution)/shard_map/attention/pallas_call | solution.py:586
  31.1 12.4 %collective-permute-done.4.top_ref = bf16[128,512]{1,0:T(8,128)(2,1)S(1)} collective-permute-done((bf16[128,512]{1,0:T(8,128)(2,1)S(1)}, bf16[128,512]{1,0:T(8,128)(2,1)S(1)}, u32[]{:S(2)}, u32[]{:S(2)}) %collective-permute-start.4) | collective-permute-done | bytes 131104 | tf_op jit(solution)/shard_map/ppermute | solution.py:644
  45.0 1.6 %collective-permute-done.5.bottom_ref = bf16[128,512]{1,0:T(8,128)(2,1)S(1)} collective-permute-done((bf16[128,512]{1,0:T(8,128)(2,1)S(1)}, bf16[128,512]{1,0:T(8,128)(2,1)S(1)}, u32[]{:S(2)}, u32[]{:S(2)}) %collective-permute-start.5) | collective-permute-done | bytes 131104 | tf_op jit(solution)/shard_map/ppermute | solution.py:644
  46.5 1.6 %collective-permute-start.2 = (bf16[512,256]{1,0:T(8,128)(2,1)S(1)}, bf16[512,256]{1,0:T(8,128)(2,1)S(1)}, u32[]{:S(2)}, u32[]{:S(2)}) collective-permute-start(bf16[512,256]{1,0:T(8,128)(2,1)S(1)} %attention.1.refs_0_), channel_id=1, source_target_pairs={{0,2},{1,3},{2,0},{3,1},{4,5},{5,4},{6,7},{7,6},{8,10},{9,11},{10,... | collective-permute-start | bytes 786440 | tf_op jit(solution)/shard_map/ppermute | solution.py:641
  48.1 1.5 %collective-permute-start.17 = (bf16[256,512]{1,0:T(8,128)(2,1)S(1)}, bf16[256,512]{1,0:T(8,128)(2,1)S(1)}, u32[]{:S(2)}, u32[]{:S(2)}) collective-permute-start(bf16[256,512]{1,0:T(8,128)(2,1)S(1)} %join.3.refs_0_), channel_id=1, source_target_pairs={{0,1},{1,0},{2,3},{3,2},{4,6},{5,7},{6,4},{7,5},{8,9},{9,8},{10,11... | collective-permute-start | bytes 786440 | tf_op jit(solution)/shard_map/ppermute | solution.py:641
  49.7 6.4 %experts.4 = (bf16[1,2048,1024]{2,1,0:T(8,128)(2,1)S(1)}, bf16[1,2048,1024]{2,1,0:T(8,128)(2,1)S(1)}, bf16[1,1024,2048]{2,1,0:T(8,128)(2,1)S(1)}, bf16[256,512]{...) custom-call(bf16[128,2048]{1,0:T(8,128)(2,1)S(1)} %get-tuple-element, ...), custom_call_target="tpu_custom_call" | custom-call | flops 3221225472 | bytes 12582912 | tf_op jit(solution)/shard_map/experts/pallas_call | solution.py:352
  59.0 3.5 %experts.7 = (bf16[256,512]{1,0:T(8,128)(2,1)S(1)}, bf16[256,512]{1,0:T(8,128)(2,1)S(1)}, bf16[256,512]{1,0:T(8,128)(2,1)S(1)}, bf16[256,512]{1,0:T(8,128)(2,1)S(1)}) custom-call(bf16[128,2048]{1,0:T(8,128)(2,1)S(1)} %collective-permute-done.25.refs_0_, bf16[128,2048]{1,0:T(8,128)(2,1)S(1)} %collective-permute-done.26.refs_1_, ...), custom_call_target="tpu_custom_call" | custom-call | flops 3221225472 | bytes 12582912 | tf_op jit(solution)/shard_map/experts/pallas_call | solution.py:352
  68.4 3.7 %experts.6 = (bf16[256,512]{1,0:T(8,128)(2,1)S(1)}, bf16[256,512]{1,0:T(8,128)(2,1)S(1)}, bf16[256,512]{1,0:T(8,128)(2,1)S(1)}, bf16[256,512]{1,0:T(8,128)(2,1)S(1)}) custom-call(bf16[256,512]{1,0:T(8,128)(2,1)S(1)} %join.3.refs_0_, bf16[256,512]{1,0:T(8,128)(2,1)S(1)} %collective-permute-done.17.refs_1_, ...), custom_call_target="tpu_custom_call" | custom-call | flops 3221225472 | bytes 12582912 | tf_op jit(solution)/shard_map/experts/pallas_call | solution.py:352
  72.1 2.3 %collective-permute-start.27 = (bf16[256,512]{1,0:T(8,128)(2,1)S(1)}, bf16[256,512]{1,0:T(8,128)(2,1)S(1)}, u32[]{:S(2)}, u32[]{:S(2)}) collective-permute-start(bf16[256,512]{1,0:T(8,128)(2,1)S(1)} %get-tuple-element.75), channel_id=1, source_target_pairs={{0,1},{1,0},{2,3},{3,2},{4,6},{5,7},{6,4},{7,5},{8,9},{9,8},{10,11... | collective-permute-start | bytes 786440 | tf_op jit(solution)/shard_map/ppermute | solution.py:641
  74.4 2.4 %collective-permute-done.8.refs_3_ = bf16[256,512]{1,0:T(8,128)(2,1)S(1)} collective-permute-done((bf16[256,512]{1,0:T(8,128)(2,1)S(1)}, bf16[256,512]{1,0:T(8,128)(2,1)S(1)}, u32[]{:S(2)}, u32[]{:S(2)}) %collective-permute-start.8) | collective-permute-done | bytes 262176 | tf_op jit(solution)/shard_map/ppermute | solution.py:641
  76.9 3.2 %collective-permute-start.21 = (bf16[256,512]{1,0:T(8,128)(2,1)S(1)}, bf16[256,512]{1,0:T(8,128)(2,1)S(1)}, u32[]{:S(2)}, u32[]{:S(2)}) collective-permute-start(bf16[256,512]{1,0:T(8,128)(2,1)S(1)} %get-tuple-element.66), channel_id=1, source_target_pairs={{0,1},{1,0},{2,3},{3,2},{4,6},{5,7},{6,4},{7,5},{8,9},{9,8},{10,11... | collective-permute-start | bytes 786440 | tf_op jit(solution)/shard_map/ppermute | solution.py:641
  80.0 3.5 %experts.5 = (bf16[256,512]{1,0:T(8,128)(2,1)S(1)}, bf16[256,512]{1,0:T(8,128)(2,1)S(1)}, bf16[256,512]{1,0:T(8,128)(2,1)S(1)}, bf16[256,512]{1,0:T(8,128)(2,1)S(1)}) custom-call(bf16[256,512]{1,0:T(8,128)(2,1)S(1)} %join.2.refs_0_, bf16[256,512]{1,0:T(8,128)(2,1)S(1)} %collective-permute-done.6.refs_1_, ...), custom_call_target="tpu_custom_call" | custom-call | flops 3221225472 | bytes 12582912 | tf_op jit(solution)/shard_map/experts/pallas_call | solution.py:352
  83.7 2.0 %collective-permute-start.33 = (bf16[256,512]{1,0:T(8,128)(2,1)S(1)}, bf16[256,512]{1,0:T(8,128)(2,1)S(1)}, u32[]{:S(2)}, u32[]{:S(2)}) collective-permute-start(bf16[256,512]{1,0:T(8,128)(2,1)S(1)} %get-tuple-element.83), channel_id=1, source_target_pairs={{0,1},{1,0},{2,3},{3,2},{4,6},{5,7},{6,4},{7,5},{8,9},{9,8},{10,11... | collective-permute-start | bytes 786440 | tf_op jit(solution)/shard_map/ppermute | solution.py:641
  85.8 1.9 %collective-permute-start.20 = (bf16[256,512]{1,0:T(8,128)(2,1)S(1)}, bf16[256,512]{1,0:T(8,128)(2,1)S(1)}, u32[]{:S(2)}, u32[]{:S(2)}) collective-permute-start(bf16[256,512]{1,0:T(8,128)(2,1)S(1)} %get-tuple-element.64), channel_id=1, source_target_pairs={{0,1},{1,0},{2,3},{3,2},{4,6},{5,7},{6,4},{7,5},{8,9},{9,8},{10,11... | collective-permute-start | bytes 786440 | tf_op jit(solution)/shard_map/ppermute | solution.py:641
  89.3 2.9 %collective-permute-done.11.near_ref = bf16[256,512]{1,0:T(8,128)(2,1)S(1)} collective-permute-done((bf16[256,512]{1,0:T(8,128)(2,1)S(1)}, bf16[256,512]{1,0:T(8,128)(2,1)S(1)}, u32[]{:S(2)}, u32[]{:S(2)}) %collective-permute-start.11) | collective-permute-done | bytes 262176 | tf_op jit(solution)/shard_map/ppermute | solution.py:641
  92.9 4.9 %collective-permute-done.33.near_ref = bf16[256,512]{1,0:T(8,128)(2,1)S(1)} collective-permute-done((bf16[256,512]{1,0:T(8,128)(2,1)S(1)}, bf16[256,512]{1,0:T(8,128)(2,1)S(1)}, u32[]{:S(2)}, u32[]{:S(2)}) %collective-permute-start.33) | collective-permute-done | bytes 262176 | tf_op jit(solution)/shard_map/ppermute | solution.py:641
  97.9 5.5 %collective-permute-done.32.near_ref = bf16[256,512]{1,0:T(8,128)(2,1)S(1)} collective-permute-done((bf16[256,512]{1,0:T(8,128)(2,1)S(1)}, bf16[256,512]{1,0:T(8,128)(2,1)S(1)}, u32[]{:S(2)}, u32[]{:S(2)}) %collective-permute-start.32) | collective-permute-done | bytes 262176 | tf_op jit(solution)/shard_map/ppermute | solution.py:641
  103.5 5.5 %collective-permute-done.20.near_ref = bf16[256,512]{1,0:T(8,128)(2,1)S(1)} collective-permute-done((bf16[256,512]{1,0:T(8,128)(2,1)S(1)}, bf16[256,512]{1,0:T(8,128)(2,1)S(1)}, u32[]{:S(2)}, u32[]{:S(2)}) %collective-permute-start.20) | collective-permute-done | bytes 262176 | tf_op jit(solution)/shard_map/ppermute | solution.py:641
  109.1 2.0 %collective-permute-start.3 = (bf16[512,256]{1,0:T(8,128)(2,1)S(1)}, bf16[512,256]{1,0:T(8,128)(2,1)S(1)}, u32[]{:S(2)}, u32[]{:S(2)}) collective-permute-start(bf16[512,256]{1,0:T(8,128)(2,1)S(1)} %collective-permute-done.1.refs_1_), channel_id=1, source_target_pairs={{0,2},{1,3},{2,0},{3,1},{4,5},{5,4},{6,7},{7,6},{8,10},{9,11},{10,... | collective-permute-start | bytes 786440 | tf_op jit(solution)/shard_map/ppermute | solution.py:641
  111.2 2.5 %collective-permute-done.10.near_ref = bf16[256,512]{1,0:T(8,128)(2,1)S(1)} collective-permute-done((bf16[256,512]{1,0:T(8,128)(2,1)S(1)}, bf16[256,512]{1,0:T(8,128)(2,1)S(1)}, u32[]{:S(2)}, u32[]{:S(2)}) %collective-permute-start.10) | collective-permute-done | bytes 262176 | tf_op jit(solution)/shard_map/ppermute | solution.py:641
  113.8 2.5 %collective-permute-start.13 = (bf16[128,512]{1,0:T(8,128)(2,1)S(1)}, bf16[128,512]{1,0:T(8,128)(2,1)S(1)}, u32[]{:S(2)}, u32[]{:S(2)}) collective-permute-start(bf16[128,512]{1,0:T(8,128)(2,1)S(1)} %get-tuple-element.59), channel_id=1, source_target_pairs={{0,24},{4,28},{8,16},{12,20},{16,8},{20,12},{24,0},{28,4},{1,25},{... | collective-permute-start | bytes 393224 | tf_op jit(solution)/shard_map/ppermute | solution.py:644
  116.4 3.7 %collective-permute-start.14 = (bf16[128,512]{1,0:T(8,128)(2,1)S(1)}, bf16[128,512]{1,0:T(8,128)(2,1)S(1)}, u32[]{:S(2)}, u32[]{:S(2)}) collective-permute-start(bf16[128,512]{1,0:T(8,128)(2,1)S(1)} %get-tuple-element.60), channel_id=1, source_target_pairs={{0,28},{4,24},{8,20},{12,16},{16,12},{20,8},{24,4},{28,0},{1,29},{... | collective-permute-start | bytes 393224 | tf_op jit(solution)/shard_map/ppermute | solution.py:644
  120.4 10.1 %collective-permute-done.23.refs_4_ = bf16[128,512]{1,0:T(8,128)(2,1)S(1)} collective-permute-done((bf16[128,512]{1,0:T(8,128)(2,1)S(1)}, bf16[128,512]{1,0:T(8,128)(2,1)S(1)}, u32[]{:S(2)}, u32[]{:S(2)}) %collective-permute-start.23) | collective-permute-done | bytes 131104 | tf_op jit(solution)/shard_map/ppermute | solution.py:644
  130.5 2.6 %collective-permute-start.35 = (bf16[128,512]{1,0:T(8,128)(2,1)S(1)}, bf16[128,512]{1,0:T(8,128)(2,1)S(1)}, u32[]{:S(2)}, u32[]{:S(2)}) collective-permute-start(bf16[128,512]{1,0:T(8,128)(2,1)S(1)} %get-tuple-element.85), channel_id=1, source_target_pairs={{0,4},{4,0},{8,12},{12,8},{16,20},{20,16},{24,28},{28,24},{1,5},{5... | collective-permute-start | bytes 393224 | tf_op jit(solution)/shard_map/ppermute | solution.py:644
  134.6 1.7 %combine.1 = (f32[256,512]{1,0:T(8,128)S(1)}, bf16[256,512]{1,0:T(8,128)(2,1)S(1)}, bf16[256,512]{1,0:T(8,128)(2,1)S(1)}) custom-call(s32[2,256]{1,0:T(2,128)S(1)} %bitcast.4, f32[2,256]{1,0:T(2,128)S(1)} %bitcast.5, bf16[128,512]{1,0:T(8,128)(2,1)S(1)} %collective-permute-done.13.refs_2_, bf16[128,512]{1,0:T(8,128)(2,1)S(1)} %collective-permute-done.14.refs_3_, ...), custom_call_target="tpu_custom_call" | custom-call | flops 268435456 | bytes 2097152 | tf_op jit(solution)/shard_map/combine/pallas_call | solution.py:474
  (69 shorter events, 19.1 us)
Async XLA Ops:
  3.3 44.8 %collective-permute-start.9 = (bf16[128,2048]{1,0:T(8,128)(2,1)S(1)}, bf16[128,2048]{1,0:T(8,128)(2,1)S(1)}, u32[]{:S(2)}, u32[]{:S(2)}) collective-permute-start(bf16[128,2048]{1,0:T(8,128)(2,1)S(1)} %get-tuple-element.51), channel_id=1, source_target_pairs={{0,4},{4,0},{8,12},{12,8},{16,20},{20,16},{24,28},{28,24},{1,5},{5... | collective-permute-start | bytes 1572872 | tf_op jit(solution)/shard_map/ppermute | solution.py:644
  3.8 8.5 %collective-permute-start = (bf16[128,256]{1,0:T(8,128)(2,1)S(1)}, bf16[128,256]{1,0:T(8,128)(2,1)S(1)}, u32[]{:S(2)}, u32[]{:S(2)}) collective-permute-start(bf16[128,256]{1,0:T(8,128)(2,1)S(1)} %get-tuple-element.47), channel_id=1, source_target_pairs={{0,4},{4,8},{8,12},{12,16},{16,20},{20,24},{24,28},{1,5},{5,9},{9,... | collective-permute-start | bytes 196616 | tf_op jit(solution)/shard_map/ppermute | solution.py:25
  5.8 13.6 %collective-permute-start.15 = (bf16[128,512]{1,0:T(8,128)(2,1)S(1)}, bf16[128,512]{1,0:T(8,128)(2,1)S(1)}, u32[]{:S(2)}, u32[]{:S(2)}) collective-permute-start(bf16[128,512]{1,0:T(8,128)(2,1)S(1)} %get-tuple-element.61), channel_id=1, source_target_pairs={{0,16},{4,20},{8,24},{12,28},{16,0},{20,4},{24,8},{28,12},{1,17},{... | collective-permute-start | bytes 393224 | tf_op jit(solution)/shard_map/ppermute | solution.py:644
  9.9 14.0 %collective-permute-start.16 = (bf16[128,512]{1,0:T(8,128)(2,1)S(1)}, bf16[128,512]{1,0:T(8,128)(2,1)S(1)}, u32[]{:S(2)}, u32[]{:S(2)}) collective-permute-start(bf16[128,512]{1,0:T(8,128)(2,1)S(1)} %get-tuple-element.62), channel_id=1, source_target_pairs={{0,20},{4,16},{8,28},{12,24},{16,4},{20,0},{24,12},{28,8},{1,21},{... | collective-permute-start | bytes 393224 | tf_op jit(solution)/shard_map/ppermute | solution.py:644
  10.8 46.3 %collective-permute-start.25 = (bf16[128,2048]{1,0:T(8,128)(2,1)S(1)}, bf16[128,2048]{1,0:T(8,128)(2,1)S(1)}, u32[]{:S(2)}, u32[]{:S(2)}) collective-permute-start(bf16[128,2048]{1,0:T(8,128)(2,1)S(1)} %get-tuple-element.72), channel_id=1, source_target_pairs={{0,8},{4,12},{8,0},{12,4},{16,24},{20,28},{24,16},{28,20},{1,9},{5... | collective-permute-start | bytes 1572872 | tf_op jit(solution)/shard_map/ppermute | solution.py:644
  12.3 46.2 %collective-permute-start.26 = (bf16[128,2048]{1,0:T(8,128)(2,1)S(1)}, bf16[128,2048]{1,0:T(8,128)(2,1)S(1)}, u32[]{:S(2)}, u32[]{:S(2)}) collective-permute-start(bf16[128,2048]{1,0:T(8,128)(2,1)S(1)} %get-tuple-element.73), channel_id=1, source_target_pairs={{0,12},{4,8},{8,4},{12,0},{16,28},{20,24},{24,20},{28,16},{1,13},{... | collective-permute-start | bytes 1572872 | tf_op jit(solution)/shard_map/ppermute | solution.py:644
  19.4 24.1 %collective-permute-start.4 = (bf16[128,512]{1,0:T(8,128)(2,1)S(1)}, bf16[128,512]{1,0:T(8,128)(2,1)S(1)}, u32[]{:S(2)}, u32[]{:S(2)}) collective-permute-start(bf16[128,512]{1,0:T(8,128)(2,1)S(1)} %get-tuple-element.48), channel_id=1, source_target_pairs={{0,24},{4,28},{8,16},{12,20},{16,8},{20,12},{24,0},{28,4},{1,25},{... | collective-permute-start | bytes 393224 | tf_op jit(solution)/shard_map/ppermute | solution.py:644
  23.9 22.6 %collective-permute-start.5 = (bf16[128,512]{1,0:T(8,128)(2,1)S(1)}, bf16[128,512]{1,0:T(8,128)(2,1)S(1)}, u32[]{:S(2)}, u32[]{:S(2)}) collective-permute-start(bf16[128,512]{1,0:T(8,128)(2,1)S(1)} %get-tuple-element.49), channel_id=1, source_target_pairs={{0,28},{4,24},{8,20},{12,16},{16,12},{20,8},{24,4},{28,0},{1,29},{... | collective-permute-start | bytes 393224 | tf_op jit(solution)/shard_map/ppermute | solution.py:644
  43.5 40.1 %collective-permute-start.1 = (bf16[512,256]{1,0:T(8,128)(2,1)S(1)}, bf16[512,256]{1,0:T(8,128)(2,1)S(1)}, u32[]{:S(2)}, u32[]{:S(2)}) collective-permute-start(bf16[512,256]{1,0:T(8,128)(2,1)S(1)} %attention.1.refs_0_), channel_id=1, source_target_pairs={{0,1},{1,0},{2,3},{3,2},{4,6},{5,7},{6,4},{7,5},{8,9},{9,8},{10,11... | collective-permute-start | bytes 786440 | tf_op jit(solution)/shard_map/ppermute | solution.py:641
  46.5 37.2 %collective-permute-start.2 = (bf16[512,256]{1,0:T(8,128)(2,1)S(1)}, bf16[512,256]{1,0:T(8,128)(2,1)S(1)}, u32[]{:S(2)}, u32[]{:S(2)}) collective-permute-start(bf16[512,256]{1,0:T(8,128)(2,1)S(1)} %attention.1.refs_0_), channel_id=1, source_target_pairs={{0,2},{1,3},{2,0},{3,1},{4,5},{5,4},{6,7},{7,6},{8,10},{9,11},{10,... | collective-permute-start | bytes 786440 | tf_op jit(solution)/shard_map/ppermute | solution.py:641
  48.1 7.9 %collective-permute-start.17 = (bf16[256,512]{1,0:T(8,128)(2,1)S(1)}, bf16[256,512]{1,0:T(8,128)(2,1)S(1)}, u32[]{:S(2)}, u32[]{:S(2)}) collective-permute-start(bf16[256,512]{1,0:T(8,128)(2,1)S(1)} %join.3.refs_0_), channel_id=1, source_target_pairs={{0,1},{1,0},{2,3},{3,2},{4,6},{5,7},{6,4},{7,5},{8,9},{9,8},{10,11... | collective-permute-start | bytes 786440 | tf_op jit(solution)/shard_map/ppermute | solution.py:641
  57.0 9.2 %collective-permute-start.6 = (bf16[256,512]{1,0:T(8,128)(2,1)S(1)}, bf16[256,512]{1,0:T(8,128)(2,1)S(1)}, u32[]{:S(2)}, u32[]{:S(2)}) collective-permute-start(bf16[256,512]{1,0:T(8,128)(2,1)S(1)} %join.2.refs_0_), channel_id=1, source_target_pairs={{0,1},{1,0},{2,3},{3,2},{4,6},{5,7},{6,4},{7,5},{8,9},{9,8},{10,11... | collective-permute-start | bytes 786440 | tf_op jit(solution)/shard_map/ppermute | solution.py:641
  58.5 8.8 %collective-permute-start.19 = (bf16[256,512]{1,0:T(8,128)(2,1)S(1)}, bf16[256,512]{1,0:T(8,128)(2,1)S(1)}, u32[]{:S(2)}, u32[]{:S(2)}) collective-permute-start(bf16[256,512]{1,0:T(8,128)(2,1)S(1)} %collective-permute-done.17.refs_1_), channel_id=1, source_target_pairs={{0,2},{1,3},{2,0},{3,1},{4,5},{5,4},{6,7},{7,6},{8,10},{9,11},{10,... | collective-permute-start | bytes 786440 | tf_op jit(solution)/shard_map/ppermute | solution.py:641
  63.9 8.2 %collective-permute-start.7 = (bf16[256,512]{1,0:T(8,128)(2,1)S(1)}, bf16[256,512]{1,0:T(8,128)(2,1)S(1)}, u32[]{:S(2)}, u32[]{:S(2)}) collective-permute-start(bf16[256,512]{1,0:T(8,128)(2,1)S(1)} %join.2.refs_0_), channel_id=1, source_target_pairs={{0,2},{1,3},{2,0},{3,1},{4,5},{5,4},{6,7},{7,6},{8,10},{9,11},{10,... | collective-permute-start | bytes 786440 | tf_op jit(solution)/shard_map/ppermute | solution.py:641
  66.2 10.7 %collective-permute-start.8 = (bf16[256,512]{1,0:T(8,128)(2,1)S(1)}, bf16[256,512]{1,0:T(8,128)(2,1)S(1)}, u32[]{:S(2)}, u32[]{:S(2)}) collective-permute-start(bf16[256,512]{1,0:T(8,128)(2,1)S(1)} %collective-permute-done.6.refs_1_), channel_id=1, source_target_pairs={{0,2},{1,3},{2,0},{3,1},{4,5},{5,4},{6,7},{7,6},{8,10},{9,11},{10,... | collective-permute-start | bytes 786440 | tf_op jit(solution)/shard_map/ppermute | solution.py:641
  67.3 18.4 %collective-permute-start.28 = (bf16[256,512]{1,0:T(8,128)(2,1)S(1)}, bf16[256,512]{1,0:T(8,128)(2,1)S(1)}, u32[]{:S(2)}, u32[]{:S(2)}) collective-permute-start(bf16[256,512]{1,0:T(8,128)(2,1)S(1)} %get-tuple-element.77), channel_id=1, source_target_pairs={{0,1},{1,0},{2,3},{3,2},{4,6},{5,7},{6,4},{7,5},{8,9},{9,8},{10,11... | collective-permute-start | bytes 786440 | tf_op jit(solution)/shard_map/ppermute | solution.py:641
  72.1 15.7 %collective-permute-start.27 = (bf16[256,512]{1,0:T(8,128)(2,1)S(1)}, bf16[256,512]{1,0:T(8,128)(2,1)S(1)}, u32[]{:S(2)}, u32[]{:S(2)}) collective-permute-start(bf16[256,512]{1,0:T(8,128)(2,1)S(1)} %get-tuple-element.75), channel_id=1, source_target_pairs={{0,1},{1,0},{2,3},{3,2},{4,6},{5,7},{6,4},{7,5},{8,9},{9,8},{10,11... | collective-permute-start | bytes 786440 | tf_op jit(solution)/shard_map/ppermute | solution.py:641
  76.9 8.9 %collective-permute-start.21 = (bf16[256,512]{1,0:T(8,128)(2,1)S(1)}, bf16[256,512]{1,0:T(8,128)(2,1)S(1)}, u32[]{:S(2)}, u32[]{:S(2)}) collective-permute-start(bf16[256,512]{1,0:T(8,128)(2,1)S(1)} %get-tuple-element.66), channel_id=1, source_target_pairs={{0,1},{1,0},{2,3},{3,2},{4,6},{5,7},{6,4},{7,5},{8,9},{9,8},{10,11... | collective-permute-start | bytes 786440 | tf_op jit(solution)/shard_map/ppermute | solution.py:641
  83.6 8.6 %collective-permute-start.11 = (bf16[256,512]{1,0:T(8,128)(2,1)S(1)}, bf16[256,512]{1,0:T(8,128)(2,1)S(1)}, u32[]{:S(2)}, u32[]{:S(2)}) collective-permute-start(bf16[256,512]{1,0:T(8,128)(2,1)S(1)} %get-tuple-element.58), channel_id=1, source_target_pairs={{0,1},{1,0},{2,3},{3,2},{4,6},{5,7},{6,4},{7,5},{8,9},{9,8},{10,11... | collective-permute-start | bytes 786440 | tf_op jit(solution)/shard_map/ppermute | solution.py:641
  83.7 14.1 %collective-permute-start.33 = (bf16[256,512]{1,0:T(8,128)(2,1)S(1)}, bf16[256,512]{1,0:T(8,128)(2,1)S(1)}, u32[]{:S(2)}, u32[]{:S(2)}) collective-permute-start(bf16[256,512]{1,0:T(8,128)(2,1)S(1)} %get-tuple-element.83), channel_id=1, source_target_pairs={{0,1},{1,0},{2,3},{3,2},{4,6},{5,7},{6,4},{7,5},{8,9},{9,8},{10,11... | collective-permute-start | bytes 786440 | tf_op jit(solution)/shard_map/ppermute | solution.py:641
  85.7 17.7 %collective-permute-start.32 = (bf16[256,512]{1,0:T(8,128)(2,1)S(1)}, bf16[256,512]{1,0:T(8,128)(2,1)S(1)}, u32[]{:S(2)}, u32[]{:S(2)}) collective-permute-start(bf16[256,512]{1,0:T(8,128)(2,1)S(1)} %get-tuple-element.81), channel_id=1, source_target_pairs={{0,1},{1,0},{2,3},{3,2},{4,6},{5,7},{6,4},{7,5},{8,9},{9,8},{10,11... | collective-permute-start | bytes 786440 | tf_op jit(solution)/shard_map/ppermute | solution.py:641
  85.8 23.3 %collective-permute-start.20 = (bf16[256,512]{1,0:T(8,128)(2,1)S(1)}, bf16[256,512]{1,0:T(8,128)(2,1)S(1)}, u32[]{:S(2)}, u32[]{:S(2)}) collective-permute-start(bf16[256,512]{1,0:T(8,128)(2,1)S(1)} %get-tuple-element.64), channel_id=1, source_target_pairs={{0,1},{1,0},{2,3},{3,2},{4,6},{5,7},{6,4},{7,5},{8,9},{9,8},{10,11... | collective-permute-start | bytes 786440 | tf_op jit(solution)/shard_map/ppermute | solution.py:641
  87.8 21.2 %collective-permute-start.22 = (bf16[256,512]{1,0:T(8,128)(2,1)S(1)}, bf16[256,512]{1,0:T(8,128)(2,1)S(1)}, u32[]{:S(2)}, u32[]{:S(2)}) collective-permute-start(bf16[256,512]{1,0:T(8,128)(2,1)S(1)} %fold.5), channel_id=1, source_target_pairs={{0,2},{1,3},{2,0},{3,1},{4,5},{5,4},{6,7},{7,6},{8,10},{9,11},{10,... | collective-permute-start | bytes 786440 | tf_op jit(solution)/shard_map/ppermute | solution.py:641
  92.2 21.5 %collective-permute-start.10 = (bf16[256,512]{1,0:T(8,128)(2,1)S(1)}, bf16[256,512]{1,0:T(8,128)(2,1)S(1)}, u32[]{:S(2)}, u32[]{:S(2)}) collective-permute-start(bf16[256,512]{1,0:T(8,128)(2,1)S(1)} %get-tuple-element.56), channel_id=1, source_target_pairs={{0,1},{1,0},{2,3},{3,2},{4,6},{5,7},{6,4},{7,5},{8,9},{9,8},{10,11... | collective-permute-start | bytes 786440 | tf_op jit(solution)/shard_map/ppermute | solution.py:641
  97.8 15.9 %collective-permute-start.12 = (bf16[256,512]{1,0:T(8,128)(2,1)S(1)}, bf16[256,512]{1,0:T(8,128)(2,1)S(1)}, u32[]{:S(2)}, u32[]{:S(2)}) collective-permute-start(bf16[256,512]{1,0:T(8,128)(2,1)S(1)} %fold.4), channel_id=1, source_target_pairs={{0,2},{1,3},{2,0},{3,1},{4,5},{5,4},{6,7},{7,6},{8,10},{9,11},{10,... | collective-permute-start | bytes 786440 | tf_op jit(solution)/shard_map/ppermute | solution.py:641
  103.4 10.4 %collective-permute-start.29 = (bf16[256,512]{1,0:T(8,128)(2,1)S(1)}, bf16[256,512]{1,0:T(8,128)(2,1)S(1)}, u32[]{:S(2)}, u32[]{:S(2)}) collective-permute-start(bf16[256,512]{1,0:T(8,128)(2,1)S(1)} %fold.6), channel_id=1, source_target_pairs={{0,2},{1,3},{2,0},{3,1},{4,5},{5,4},{6,7},{7,6},{8,10},{9,11},{10,... | collective-permute-start | bytes 786440 | tf_op jit(solution)/shard_map/ppermute | solution.py:641
  109.1 11.2 %collective-permute-start.3 = (bf16[512,256]{1,0:T(8,128)(2,1)S(1)}, bf16[512,256]{1,0:T(8,128)(2,1)S(1)}, u32[]{:S(2)}, u32[]{:S(2)}) collective-permute-start(bf16[512,256]{1,0:T(8,128)(2,1)S(1)} %collective-permute-done.1.refs_1_), channel_id=1, source_target_pairs={{0,2},{1,3},{2,0},{3,1},{4,5},{5,4},{6,7},{7,6},{8,10},{9,11},{10,... | collective-permute-start | bytes 786440 | tf_op jit(solution)/shard_map/ppermute | solution.py:641
  113.7 16.8 %collective-permute-start.23 = (bf16[128,512]{1,0:T(8,128)(2,1)S(1)}, bf16[128,512]{1,0:T(8,128)(2,1)S(1)}, u32[]{:S(2)}, u32[]{:S(2)}) collective-permute-start(bf16[128,512]{1,0:T(8,128)(2,1)S(1)} %get-tuple-element.67), channel_id=1, source_target_pairs={{0,16},{4,20},{8,24},{12,28},{16,0},{20,4},{24,8},{28,12},{1,17},{... | collective-permute-start | bytes 393224 | tf_op jit(solution)/shard_map/ppermute | solution.py:644
  113.7 16.8 %collective-permute-start.24 = (bf16[128,512]{1,0:T(8,128)(2,1)S(1)}, bf16[128,512]{1,0:T(8,128)(2,1)S(1)}, u32[]{:S(2)}, u32[]{:S(2)}) collective-permute-start(bf16[128,512]{1,0:T(8,128)(2,1)S(1)} %get-tuple-element.68), channel_id=1, source_target_pairs={{0,20},{4,16},{8,28},{12,24},{16,4},{20,0},{24,12},{28,8},{1,21},{... | collective-permute-start | bytes 393224 | tf_op jit(solution)/shard_map/ppermute | solution.py:644
  113.8 20.8 %collective-permute-start.13 = (bf16[128,512]{1,0:T(8,128)(2,1)S(1)}, bf16[128,512]{1,0:T(8,128)(2,1)S(1)}, u32[]{:S(2)}, u32[]{:S(2)}) collective-permute-start(bf16[128,512]{1,0:T(8,128)(2,1)S(1)} %get-tuple-element.59), channel_id=1, source_target_pairs={{0,24},{4,28},{8,16},{12,20},{16,8},{20,12},{24,0},{28,4},{1,25},{... | collective-permute-start | bytes 393224 | tf_op jit(solution)/shard_map/ppermute | solution.py:644
  116.4 18.3 %collective-permute-start.14 = (bf16[128,512]{1,0:T(8,128)(2,1)S(1)}, bf16[128,512]{1,0:T(8,128)(2,1)S(1)}, u32[]{:S(2)}, u32[]{:S(2)}) collective-permute-start(bf16[128,512]{1,0:T(8,128)(2,1)S(1)} %get-tuple-element.60), channel_id=1, source_target_pairs={{0,28},{4,24},{8,20},{12,16},{16,12},{20,8},{24,4},{28,0},{1,29},{... | collective-permute-start | bytes 393224 | tf_op jit(solution)/shard_map/ppermute | solution.py:644
  120.3 16.1 %collective-permute-start.30 = (bf16[128,512]{1,0:T(8,128)(2,1)S(1)}, bf16[128,512]{1,0:T(8,128)(2,1)S(1)}, u32[]{:S(2)}, u32[]{:S(2)}) collective-permute-start(bf16[128,512]{1,0:T(8,128)(2,1)S(1)} %get-tuple-element.78), channel_id=1, source_target_pairs={{0,8},{4,12},{8,0},{12,4},{16,24},{20,28},{24,16},{28,20},{1,9},{5... | collective-permute-start | bytes 393224 | tf_op jit(solution)/shard_map/ppermute | solution.py:644
  (9 other events, 171.4 us)
